TPU v7x, 32 devices: a whole 2x2x4 slice. The times are simulated.
32 devices in a mesh: sp: 8 (over z, core), tp: 4 (over y, x).
Axes of the slice: x: 2, y: 2, z: 4, core: 2. Of those that a mesh axis runs over, the one named last changes fastest.
Arguments:
- residual: bfloat16 [3072, 2048], P('sp', 'tp'), may hold values from -40 to 40
- norm_gain: bfloat16 [3, 2048], P(None, 'tp'), may hold values from 0.099609375 to 1.8984375
- w_query: bfloat16 [3, 2048, 2048], P(None, 'tp'), may hold values from -2 to 2
- w_key: bfloat16 [3, 2048, 2048], P(None, 'tp'), may hold values from -8 to 8
- w_value: bfloat16 [3, 2048, 2048], P(None, 'tp'), may hold values from -0.125 to 0.125
- w_out: bfloat16 [3, 2048, 2048], P(None, 'tp'), may hold values from -0.25 to 0.25
- offset_bias: float32 [3, 32, 15, 31], P(None, 'tp'), may hold values from -5 to 5
Outputs:
- out_residual: bfloat16 [3072, 2048], P('sp', 'tp')
All inputs are finite; a program needn't handle non-finite values.
Results may differ from a plain program's by a relative error of at most 0.014.
Values may be sent and summed in bfloat16 or wider, within the bound.
A program may use at most 128 MiB of HBM per device.

v0:
```python
import jax
import jax.numpy as jnp
from jax import lax
from jax.sharding import PartitionSpec as P

HEAD_DIM = 64
GRID_W = 64
NA_ROWS = 8
NA_COLS = 16
LAYERS = 3


epsilon = 1e-06


def padded_2(array, sides, width):
    for axis, dim in sides:
        size, length = (lax.axis_size(axis), array.shape[dim])
        up = [(i, (i + 1) % size) for i in range(size - 1)]
        down = [(j, i) for i, j in up]
        last = lax.slice_in_dim(array, length - width, length, axis=dim)
        first = lax.slice_in_dim(array, 0, width, axis=dim)
        before = lax.ppermute(last, axis, up)
        after = lax.ppermute(first, axis, down)
        array = jnp.concatenate([before, array, after], axis=dim)
    return array


def shortened(array):
    return jax.tree.map(lambda a: a.astype(jnp.bfloat16) if a.dtype == jnp.float32 else a, array)


def contract(left, right):
    return lax.dot_general(
        left, right, (((1,), (1,)), ((), ())), preferred_element_type=jnp.float32
    )


def per_device(residual, norm_gain, w_query, w_key, w_value, w_out, offset_bias):
    token_count = residual.shape[0]
    local_feats = residual.shape[1]
    local_heads = offset_bias.shape[1]
    head_cols = local_heads * HEAD_DIM
    rows_dev = token_count // GRID_W
    rows_all = rows_dev * lax.axis_size("sp")
    row_base = lax.axis_index("sp") * rows_dev
    reach = NA_ROWS // 2
    slab_width = min(2 * NA_COLS, GRID_W)
    tile_starts = list(range(0, GRID_W, NA_COLS))
    slab_starts = [min(max(start - NA_COLS // 2, 0), GRID_W - slab_width) for start in tile_starts]
    tile_info = []
    for start, slab in zip(tile_starts, slab_starts):
        query_cols = start + jnp.arange(NA_COLS, dtype=jnp.int32)
        key_cols = slab + jnp.arange(slab_width, dtype=jnp.int32)
        first_col = jnp.clip(query_cols - NA_COLS // 2, 0, GRID_W - NA_COLS)
        inside = (key_cols[None, :] >= first_col[:, None]) & (
            key_cols[None, :] < first_col[:, None] + NA_COLS
        )
        offsets = key_cols[None, :] - query_cols[:, None] + (NA_COLS - 1)
        onehot = (offsets[:, :, None] == jnp.arange(2 * NA_COLS - 1, dtype=jnp.int32)).astype(
            jnp.float32
        )
        tile_info.append((start, slab, inside, onehot))
    stream = residual
    for layer_index in range(LAYERS):
        res_float = stream.astype(jnp.float32)
        gathered, gain_all = (
            lax.all_gather(stream, "tp", axis=1, tiled=True),
            lax.all_gather(norm_gain[layer_index][None, :], "tp", axis=1, tiled=True),
        )
        full_float = gathered.astype(jnp.float32)
        inverse = lax.rsqrt(jnp.mean(full_float * full_float, axis=1, keepdims=True) + epsilon)
        normed_all = (full_float * inverse * gain_all.astype(jnp.float32)).astype(jnp.bfloat16)
        queries = contract(normed_all, w_query[layer_index])
        keys = contract(normed_all, w_key[layer_index])
        values = contract(normed_all, w_value[layer_index])
        queries = queries.astype(jnp.bfloat16)
        key_value = jnp.concatenate(
            [keys.astype(jnp.bfloat16), values.astype(jnp.bfloat16)], axis=1
        )
        padded = padded_2(key_value, (("sp", 0),), reach * GRID_W)
        key_grid = padded.reshape(rows_dev + 2 * reach, GRID_W, 2, local_heads, HEAD_DIM)
        query_grid = queries.reshape(rows_dev, GRID_W, local_heads, HEAD_DIM)
        lookup = offset_bias[layer_index]

        def one_row(row_index, query_row):
            row_global = row_base + row_index
            first_row = jnp.clip(row_global - reach, 0, rows_all - NA_ROWS)
            local_first = first_row - row_base + reach
            window = lax.dynamic_slice_in_dim(key_grid, local_first, NA_ROWS, 0)
            row_offset = (
                first_row + jnp.arange(NA_ROWS, dtype=jnp.int32) - row_global + (NA_ROWS - 1)
            )
            row_onehot = (
                row_offset[:, None] == jnp.arange(2 * NA_ROWS - 1, dtype=jnp.int32)
            ).astype(jnp.float32)
            row_bias = jnp.einsum(
                "hab,ra->hrb", lookup, row_onehot, precision=lax.Precision.HIGHEST
            )
            pieces = []
            for start, slab, inside, onehot in tile_info:
                query_tile = query_row[start : start + NA_COLS]
                slab_keys = window[:, slab : slab + slab_width, 0]
                slab_values = window[:, slab : slab + slab_width, 1]
                bias_terms = jnp.einsum(
                    "hrb,wsb->hwrs", row_bias, onehot, precision=lax.Precision.HIGHEST
                )
                scores = jnp.einsum(
                    "whd,rshd->hwrs", query_tile, slab_keys, preferred_element_type=jnp.float32
                )
                scores = scores * HEAD_DIM ** (-0.5) + bias_terms
                scores = jnp.where(inside[None, :, None, :], scores, -jnp.inf)
                weights = jax.nn.softmax(
                    scores.reshape(local_heads, NA_COLS, NA_ROWS * slab_width), axis=-1
                ).astype(jnp.bfloat16)
                weights = weights.reshape(local_heads, NA_COLS, NA_ROWS, slab_width)
                attended = jnp.einsum(
                    "hwrs,rshd->whd", weights, slab_values, preferred_element_type=jnp.float32
                )
                pieces.append(attended.astype(jnp.bfloat16).reshape(NA_COLS, head_cols))
            return jnp.concatenate(pieces, axis=0)

        attended = jax.vmap(one_row)(jnp.arange(rows_dev, dtype=jnp.int32), query_grid).reshape(
            token_count, head_cols
        )
        portion = jax.tree.map(
            lambda part: lax.all_gather(part, "tp", axis=1, tiled=True), shortened(attended)
        )
        out_rows = lax.slice_in_dim(w_out[layer_index], 0, portion.shape[1], axis=1)
        mixed = jnp.zeros((token_count, local_feats), jnp.float32) + contract(portion, out_rows)
        stream = (res_float + mixed).astype(jnp.bfloat16)
    return stream


def solution(mesh):
    in_specs = (
        P("sp", "tp"),
        P(None, "tp"),
        P(None, "tp", None),
        P(None, "tp", None),
        P(None, "tp", None),
        P(None, "tp", None),
        P(None, "tp", None, None),
    )
    out_specs = P("sp", "tp")
    return jax.shard_map(
        per_device, mesh=mesh, in_specs=in_specs, out_specs=out_specs, check_vma=False
    )
```

profile of v0, /device:TPU:11, one launch (start us, length us, event | category | flops | bytes accessed | tf_op | source)
XLA Modules:
  0.0 572.4 jit_solution(9125347136476089552)
XLA Ops:
  12.0 6.1 %all_gather.28 = bf16[1,2048]{1,0:T(2,128)(2,1)S(1)} all-gather(bf16[1,512]{1,0:T(2,128)(2,1)S(1)} %get-tuple-element.75), channel_id=1, replica_groups=mesh['sp'=8,'tp'=4] {'tp'}, dimensions={1}, use_global_device_ids=true | all-gather | bytes 5120 | tf_op jit(solution)/shard_map/all_gather | solution.py:69
  20.8 3.2 fusion.350
  24.0 3.2 fusion.357
  27.2 3.1 fusion.364
  31.8 9.1 %all-gather.7.cloned.1.call-done = bf16[384,2048]{1,0:T(8,128)(2,1)} async-done(((bf16[384,512]{1,0:T(8,128)(2,1)}), bf16[384,2048]{1,0:T(8,128)(2,1)}) %all-gather.7.cloned.1.call-update) | async-done | bytes 1572880 | tf_op jit(solution)/shard_map/all_gather | solution.py:68
  42.7 3.2 fusion.207
  50.5 3.8 collective-permute-start
  54.3 13.9 %collective-permute-start.1 = (bf16[256,1024]{1,0:T(8,128)(2,1)}, bf16[256,1024]{1,0:T(8,128)(2,1)}, u32[]{:S(2)}, u32[]{:S(2)}) collective-permute-start(bf16[256,1024]{1,0:T(8,128)(2,1)} %get-tuple-element.70), channel_id=1, source_target_pairs={{4,0},{8,4},{12,8},{16,12},{20,16},{24,20},{28,24},{5,1},{9,5},{13... | collective-permute-start | bytes 1572872 | tf_op jit(solution)/shard_map/ppermute | solution.py:24
  68.2 3.4 fusion.213
  78.7 6.0 %reshape.360 = bf16[14,64,2,8,64]{4,3,2,1,0:T(8,128)(2,1)} reshape(bf16[896,1024]{1,0:T(8,128)(2,1)} %pad_maximum_fusion) | data formatting | bytes 3670016 | tf_op jit(solution)/shard_map/reshape | solution.py:82
  84.7 7.7 %broadcast.472.clone2 = bf16[6,8,64,2,8,64]{5,2,1,4,0,3:T(8,128)(2,1)} broadcast(bf16[]{:T(256)} %constant.63), dimensions={} | broadcast | bytes 6291458
  92.4 27.7 %while.3 = (s32[]{:T(128)}, bf16[14,64,2,8,64]{4,3,2,1,0:T(8,128)(2,1)}, s32[6,5]{1,0:T(8,128)}, bf16[6,8,64,2,8,64]{5,2,1,4,0,3:T(8,128)(2,1)}, s32[]{:T(128)}) while((s32[]{:T(128)}, bf16[14,64,2,8,64]{4,3,2,1,0:T(8,128)(2,1)}, s32[6,5]{1,0:T(8,128)}, bf16[6,8,64,2,8,64]{5,2,1,4,0,3:T(8,128)(2,1)}, s32[]{:T(128)}) %tuple.71), condition=%wide.while_cond, body=%wide.while_body.sunk | while | flops 2 | bytes 5243501 | solution.py:90
  120.2 7.1 %fusion.410 = (f32[6,8,16]{2,1,0:T(8,128)S(1)}, f32[6,8,16,8,32]{4,2,3,1,0:T(8,128)S(1)}) fusion(f32[16,32,6,8,8]{1,4,3,2,0:T(8,128)} %fusion.350, bf16[6,8,64,2,8,64]{5,2,1,4,0,3:T(8,128)(2,1)} %get-tuple-element.12, bf16[6,16,8,64]{3,2,1,0:T(8,128)(2,1)S(1)} %copy-done.16, pred[16,32]{1,0:T(8,128)(4,1)S(1)} %copy-done.44), kind=kOutput, calls=%fused_computation.379 | convolution fusion | flops 25951488 | bytes 7179776 | tf_op jit(solution)/shard_map/vmap(whd,rshd->hwrs)/dot_general | solution.py:108
  128.0 3.4 fusion.306
  132.3 7.1 %fusion.409 = (f32[6,8,16]{2,1,0:T(8,128)S(1)}, f32[6,8,16,8,32]{4,2,3,1,0:T(8,128)S(1)}) fusion(f32[16,32,6,8,8]{1,4,3,2,0:T(8,128)} %fusion.357, bf16[6,8,64,2,8,64]{5,2,1,4,0,3:T(8,128)(2,1)} %get-tuple-element.12, bf16[6,16,8,64]{3,2,1,0:T(8,128)(2,1)S(1)} %copy-done.13, pred[16,32]{1,0:T(8,128)(4,1)} %compare_and_fusion.2), kind=kOutput, calls=%fused_computation.378 | convolution fusion | flops 25951488 | bytes 7181312 | tf_op jit(solution)/shard_map/vmap(whd,rshd->hwrs)/dot_general | solution.py:108
  140.1 3.4 fusion.309
  144.4 7.5 %fusion.408 = (f32[6,8,16]{2,1,0:T(8,128)S(1)}, f32[6,8,16,8,32]{4,2,3,1,0:T(8,128)S(1)}) fusion(f32[16,32,6,8,8]{1,4,3,2,0:T(8,128)} %fusion.364, bf16[6,8,64,2,8,64]{5,2,1,4,0,3:T(8,128)(2,1)} %get-tuple-element.12, bf16[6,16,8,64]{3,2,1,0:T(8,128)(2,1)S(1)} %copy-done.10, pred[16,32]{1,0:T(8,128)(4,1)} %compare_and_fusion.1), kind=kOutput, calls=%fused_computation.377 | convolution fusion | flops 25951488 | bytes 7181312 | tf_op jit(solution)/shard_map/vmap(whd,rshd->hwrs)/dot_general | solution.py:108
  152.6 3.4 fusion.312
  156.9 6.2 %fusion.407 = (f32[6,8,16]{2,1,0:T(8,128)S(1)}, f32[6,8,16,8,32]{4,2,3,1,0:T(8,128)S(1)}) fusion(f32[16,32,6,8,8]{1,4,3,2,0:T(8,128)S(1)} %fusion.371, bf16[6,8,64,2,8,64]{5,2,1,4,0,3:T(8,128)(2,1)} %get-tuple-element.12, bf16[6,16,8,64]{3,2,1,0:T(8,128)(2,1)S(1)} %copy-done.7, pred[16,32]{1,0:T(8,128)(4,1)} %compare_and_fusion), kind=kOutput, calls=%fused_computation.376 | convolution fusion | flops 25951488 | bytes 4822016 | tf_op jit(solution)/shard_map/vmap(whd,rshd->hwrs)/dot_general | solution.py:108
  163.8 3.4 fusion.315
  168.4 30.6 %all-gather.9.cloned.1.call-done = bf16[384,2048]{1,0:T(8,128)(2,1)} async-done(((bf16[384,512]{1,0:T(8,128)(2,1)}), bf16[384,2048]{1,0:T(8,128)(2,1)}) %all-gather.9.cloned.1.call-update) | async-done | bytes 1572880 | tf_op jit(solution)/shard_map/all_gather | solution.py:127
  199.0 3.8 fusion.204
  202.9 5.3 all_gather.31
  209.1 3.2 fusion.348
  212.3 3.2 fusion.355
  215.5 3.1 fusion.362
  220.1 13.7 %all-gather.11.cloned.1.call-done = bf16[384,2048]{1,0:T(8,128)(2,1)} async-done(((bf16[384,512]{1,0:T(8,128)(2,1)}), bf16[384,2048]{1,0:T(8,128)(2,1)}) %all-gather.11.cloned.1.call-update) | async-done | bytes 1572880 | tf_op jit(solution)/shard_map/all_gather | solution.py:68
  235.6 3.2 fusion.219
  243.4 3.8 collective-permute-start.2
  249.1 3.4 fusion.222
  260.8 6.0 %reshape.367 = bf16[14,64,2,8,64]{4,3,2,1,0:T(8,128)(2,1)} reshape(bf16[896,1024]{1,0:T(8,128)(2,1)} %pad_maximum_fusion.1) | data formatting | bytes 3670016 | tf_op jit(solution)/shard_map/reshape | solution.py:82
  266.8 7.7 %broadcast.472.clone2.1 = bf16[6,8,64,2,8,64]{5,2,1,4,0,3:T(8,128)(2,1)} broadcast(bf16[]{:T(256)} %constant.63), dimensions={} | broadcast | bytes 6291458
  274.5 27.9 %while.4 = (s32[]{:T(128)}, bf16[14,64,2,8,64]{4,3,2,1,0:T(8,128)(2,1)}, s32[6,5]{1,0:T(8,128)}, bf16[6,8,64,2,8,64]{5,2,1,4,0,3:T(8,128)(2,1)}, s32[]{:T(128)}) while((s32[]{:T(128)}, bf16[14,64,2,8,64]{4,3,2,1,0:T(8,128)(2,1)}, s32[6,5]{1,0:T(8,128)}, bf16[6,8,64,2,8,64]{5,2,1,4,0,3:T(8,128)(2,1)}, s32[]{:T(128)}) %tuple.92), condition=%wide.while_cond.1, body=%wide.while_body.1.sunk | while | flops 2 | bytes 5243501 | solution.py:90
  302.5 7.1 %fusion.414 = (f32[6,8,16]{2,1,0:T(8,128)S(1)}, f32[6,8,16,8,32]{4,2,3,1,0:T(8,128)S(1)}) fusion(f32[16,32,6,8,8]{1,4,3,2,0:T(8,128)} %fusion.348, bf16[6,8,64,2,8,64]{5,2,1,4,0,3:T(8,128)(2,1)} %get-tuple-element.20, bf16[6,16,8,64]{3,2,1,0:T(8,128)(2,1)S(1)} %copy-done.17, pred[16,32]{1,0:T(8,128)(4,1)S(1)} %copy-done.45), kind=kOutput, calls=%fused_computation.383 | convolution fusion | flops 25951488 | bytes 7179776 | tf_op jit(solution)/shard_map/vmap(whd,rshd->hwrs)/dot_general | solution.py:108
  310.3 3.4 fusion.318
  314.6 7.1 %fusion.413 = (f32[6,8,16]{2,1,0:T(8,128)S(1)}, f32[6,8,16,8,32]{4,2,3,1,0:T(8,128)S(1)}) fusion(f32[16,32,6,8,8]{1,4,3,2,0:T(8,128)} %fusion.355, bf16[6,8,64,2,8,64]{5,2,1,4,0,3:T(8,128)(2,1)} %get-tuple-element.20, bf16[6,16,8,64]{3,2,1,0:T(8,128)(2,1)S(1)} %copy-done.14, pred[16,32]{1,0:T(8,128)(4,1)} %compare_and_fusion.2), kind=kOutput, calls=%fused_computation.382 | convolution fusion | flops 25951488 | bytes 7181312 | tf_op jit(solution)/shard_map/vmap(whd,rshd->hwrs)/dot_general | solution.py:108
  322.4 3.4 fusion.321
  326.7 7.5 %fusion.412 = (f32[6,8,16]{2,1,0:T(8,128)S(1)}, f32[6,8,16,8,32]{4,2,3,1,0:T(8,128)S(1)}) fusion(f32[16,32,6,8,8]{1,4,3,2,0:T(8,128)} %fusion.362, bf16[6,8,64,2,8,64]{5,2,1,4,0,3:T(8,128)(2,1)} %get-tuple-element.20, bf16[6,16,8,64]{3,2,1,0:T(8,128)(2,1)S(1)} %copy-done.11, pred[16,32]{1,0:T(8,128)(4,1)} %compare_and_fusion.1), kind=kOutput, calls=%fused_computation.381 | convolution fusion | flops 25951488 | bytes 7181312 | tf_op jit(solution)/shard_map/vmap(whd,rshd->hwrs)/dot_general | solution.py:108
  334.9 3.4 fusion.324
  339.2 6.2 %fusion.411 = (f32[6,8,16]{2,1,0:T(8,128)S(1)}, f32[6,8,16,8,32]{4,2,3,1,0:T(8,128)S(1)}) fusion(f32[16,32,6,8,8]{1,4,3,2,0:T(8,128)S(1)} %fusion.369, bf16[6,8,64,2,8,64]{5,2,1,4,0,3:T(8,128)(2,1)} %get-tuple-element.20, bf16[6,16,8,64]{3,2,1,0:T(8,128)(2,1)S(1)} %copy-done.8, pred[16,32]{1,0:T(8,128)(4,1)} %compare_and_fusion), kind=kOutput, calls=%fused_computation.380 | convolution fusion | flops 25951488 | bytes 4822016 | tf_op jit(solution)/shard_map/vmap(whd,rshd->hwrs)/dot_general | solution.py:108
  346.1 3.4 fusion.327
  350.7 29.5 %all-gather.13.cloned.1.call-done = bf16[384,2048]{1,0:T(8,128)(2,1)} async-done(((bf16[384,512]{1,0:T(8,128)(2,1)}), bf16[384,2048]{1,0:T(8,128)(2,1)}) %all-gather.13.cloned.1.call-update) | async-done | bytes 1572880 | tf_op jit(solution)/shard_map/all_gather | solution.py:127
  380.2 3.8 fusion.201
  384.1 5.3 all_gather.34
  390.3 3.2 fusion.346
  393.5 3.2 fusion.353
  396.7 3.1 fusion.360
  401.3 13.7 %all-gather.15.cloned.1.call-done = bf16[384,2048]{1,0:T(8,128)(2,1)} async-done(((bf16[384,512]{1,0:T(8,128)(2,1)}), bf16[384,2048]{1,0:T(8,128)(2,1)}) %all-gather.15.cloned.1.call-update) | async-done | bytes 1572880 | tf_op jit(solution)/shard_map/all_gather | solution.py:68
  416.8 3.2 fusion.228
  424.6 3.8 collective-permute-start.4
  430.3 3.4 fusion.231
  442.0 6.0 %reshape.374 = bf16[14,64,2,8,64]{4,3,2,1,0:T(8,128)(2,1)} reshape(bf16[896,1024]{1,0:T(8,128)(2,1)} %pad_maximum_fusion.2) | data formatting | bytes 3670016 | tf_op jit(solution)/shard_map/reshape | solution.py:82
  448.0 7.7 %broadcast.472.clone = bf16[6,8,64,2,8,64]{5,2,1,4,0,3:T(8,128)(2,1)} broadcast(bf16[]{:T(256)} %constant.63), dimensions={} | broadcast | bytes 6291458
  455.7 27.9 %while.5 = (s32[]{:T(128)}, bf16[14,64,2,8,64]{4,3,2,1,0:T(8,128)(2,1)}, s32[6,5]{1,0:T(8,128)}, bf16[6,8,64,2,8,64]{5,2,1,4,0,3:T(8,128)(2,1)}, s32[]{:T(128)}) while((s32[]{:T(128)}, bf16[14,64,2,8,64]{4,3,2,1,0:T(8,128)(2,1)}, s32[6,5]{1,0:T(8,128)}, bf16[6,8,64,2,8,64]{5,2,1,4,0,3:T(8,128)(2,1)}, s32[]{:T(128)}) %tuple.93), condition=%wide.while_cond.2, body=%wide.while_body.2.sunk | while | flops 2 | bytes 5243501 | solution.py:90
  483.6 7.1 %fusion.418 = (f32[6,8,16]{2,1,0:T(8,128)S(1)}, f32[6,8,16,8,32]{4,2,3,1,0:T(8,128)S(1)}) fusion(f32[16,32,6,8,8]{1,4,3,2,0:T(8,128)} %fusion.346, bf16[6,8,64,2,8,64]{5,2,1,4,0,3:T(8,128)(2,1)} %get-tuple-element.28, bf16[6,16,8,64]{3,2,1,0:T(8,128)(2,1)S(1)} %copy-done.15, pred[16,32]{1,0:T(8,128)(4,1)S(1)} %copy-done.46), kind=kOutput, calls=%fused_computation.387 | convolution fusion | flops 25951488 | bytes 7179776 | tf_op jit(solution)/shard_map/vmap(whd,rshd->hwrs)/dot_general | solution.py:108
  491.5 3.4 fusion.330
  495.8 7.1 %fusion.417 = (f32[6,8,16]{2,1,0:T(8,128)S(1)}, f32[6,8,16,8,32]{4,2,3,1,0:T(8,128)S(1)}) fusion(f32[16,32,6,8,8]{1,4,3,2,0:T(8,128)} %fusion.353, bf16[6,8,64,2,8,64]{5,2,1,4,0,3:T(8,128)(2,1)} %get-tuple-element.28, bf16[6,16,8,64]{3,2,1,0:T(8,128)(2,1)S(1)} %copy-done.12, pred[16,32]{1,0:T(8,128)(4,1)S(1)} %copy-done.43), kind=kOutput, calls=%fused_computation.386 | convolution fusion | flops 25951488 | bytes 7179776 | tf_op jit(solution)/shard_map/vmap(whd,rshd->hwrs)/dot_general | solution.py:108
  503.6 3.4 fusion.333
  507.9 7.3 %fusion.416 = (f32[6,8,16]{2,1,0:T(8,128)S(1)}, f32[6,8,16,8,32]{4,2,3,1,0:T(8,128)S(1)}) fusion(f32[16,32,6,8,8]{1,4,3,2,0:T(8,128)} %fusion.360, bf16[6,8,64,2,8,64]{5,2,1,4,0,3:T(8,128)(2,1)} %get-tuple-element.28, bf16[6,16,8,64]{3,2,1,0:T(8,128)(2,1)S(1)} %copy-done.9, pred[16,32]{1,0:T(8,128)(4,1)S(1)} %copy-done.42), kind=kOutput, calls=%fused_computation.385 | convolution fusion | flops 25951488 | bytes 7179776 | tf_op jit(solution)/shard_map/vmap(whd,rshd->hwrs)/dot_general | solution.py:108
  516.0 3.4 fusion.336
  520.2 6.2 %fusion.415 = (f32[6,8,16]{2,1,0:T(8,128)S(1)}, f32[6,8,16,8,32]{4,2,3,1,0:T(8,128)S(1)}) fusion(f32[16,32,6,8,8]{1,4,3,2,0:T(8,128)S(1)} %fusion.367, bf16[6,8,64,2,8,64]{5,2,1,4,0,3:T(8,128)(2,1)} %get-tuple-element.28, bf16[6,16,8,64]{3,2,1,0:T(8,128)(2,1)S(1)} %copy-done.6, pred[16,32]{1,0:T(8,128)(4,1)S(1)} %copy-done.41), kind=kOutput, calls=%fused_computation.384 | convolution fusion | flops 25951488 | bytes 4820480 | tf_op jit(solution)/shard_map/vmap(whd,rshd->hwrs)/dot_general | solution.py:108
  527.2 3.4 fusion.339
  531.7 29.6 %all-gather.17.cloned.1.call-done = bf16[384,2048]{1,0:T(8,128)(2,1)} async-done(((bf16[384,512]{1,0:T(8,128)(2,1)}), bf16[384,2048]{1,0:T(8,128)(2,1)}) %all-gather.17.cloned.1.call-update) | async-done | bytes 1572880 | tf_op jit(solution)/shard_map/all_gather | solution.py:127
  561.2 3.8 fusion.198
  (271 shorter events, 163.8 us)
Async XLA Ops:
  6.5 34.4 %all-gather.7.cloned.1.call-start = ((), (), s32[]{:S(2)}) async-start(), calls=%async_computation | async-start | bytes 1966080 | tf_op jit(solution)/shard_map/all_gather | solution.py:68
  7.3 191.8 %all-gather.9.cloned.1.call-start = ((), (), s32[]{:S(2)}) async-start(), calls=%async_computation.1 | async-start | bytes 1966080 | tf_op jit(solution)/shard_map/all_gather | solution.py:127
  10.5 10.1 %copy-start.38 = (s32[6,8]{1,0:T(8,128)}, s32[6,8]{1,0:T(8,128)S(1)}, u32[]{:S(2)}) copy-start(s32[6,8]{1,0:T(8,128)S(1)} %subtract_add_fusion.4) | copy-start | bytes 580
  20.8 6.4 %copy-start.32 = (s32[16,32]{1,0:T(8,128)}, s32[16,32]{1,0:T(8,128)S(1)}, u32[]{:S(2)}) copy-start(s32[16,32]{1,0:T(8,128)S(1)} %subtract_add_fusion.1) | copy-start | bytes 6148
  20.8 9.5 %copy-start.35 = (s32[16,32]{1,0:T(8,128)}, s32[16,32]{1,0:T(8,128)S(1)}, u32[]{:S(2)}) copy-start(s32[16,32]{1,0:T(8,128)S(1)} %subtract_add_fusion) | copy-start | bytes 6148
  42.7 3.3 copy-start.3
  42.7 3.3 copy-start.47
  48.6 0.7 copy-start
  50.5 25.4 %collective-permute-start = (bf16[256,1024]{1,0:T(8,128)(2,1)}, bf16[256,1024]{1,0:T(8,128)(2,1)}, u32[]{:S(2)}, u32[]{:S(2)}) collective-permute-start(bf16[256,1024]{1,0:T(8,128)(2,1)} %get-tuple-element.69), channel_id=1, source_target_pairs={{0,4},{4,8},{8,12},{12,16},{16,20},{20,24},{24,28},{1,5},{5,9},{9,... | collective-permute-start | bytes 1572872 | tf_op jit(solution)/shard_map/ppermute | solution.py:23
  54.3 21.6 %collective-permute-start.1 = (bf16[256,1024]{1,0:T(8,128)(2,1)}, bf16[256,1024]{1,0:T(8,128)(2,1)}, u32[]{:S(2)}, u32[]{:S(2)}) collective-permute-start(bf16[256,1024]{1,0:T(8,128)(2,1)} %get-tuple-element.70), channel_id=1, source_target_pairs={{4,0},{8,4},{12,8},{16,12},{20,16},{24,20},{28,24},{5,1},{9,5},{13... | collective-permute-start | bytes 1572872 | tf_op jit(solution)/shard_map/ppermute | solution.py:24
  92.4 27.7 %copy-start.16 = (bf16[6,16,8,64]{3,2,1,0:T(8,128)(2,1)S(1)}, bf16[6,16,8,64]{3,2,1,0:T(8,128)(2,1)}, u32[]{:S(2)}) copy-start(bf16[6,16,8,64]{3,2,1,0:T(8,128)(2,1)} %get-tuple-element.65) | copy-start | bytes 294916
  92.4 27.7 %copy-start.44 = (pred[16,32]{1,0:T(8,128)(4,1)S(1)}, pred[16,32]{1,0:T(8,128)(4,1)}, u32[]{:S(2)}) copy-start(pred[16,32]{1,0:T(8,128)(4,1)} %fusion.392) | copy-start | bytes 1540
  128.0 4.3 copy-start.13
  140.1 4.3 copy-start.10
  152.6 4.3 copy-start.7
  163.8 3.7 copy-start.22
  163.8 3.7 copy-start.25
  163.8 3.7 copy-start.28
  163.8 35.2 %copy-start.18 = (bf16[384,512]{1,0:T(8,128)(2,1)S(1)}, bf16[384,512]{1,0:T(8,128)(2,1)}, u32[]{:S(2)}) copy-start(bf16[384,512]{1,0:T(8,128)(2,1)} %param.7) | copy-start | bytes 1179652
  168.3 34.6 %copy-start.51 = (bf16[1,512]{1,0:T(2,128)(2,1)S(1)}, bf16[1,512]{1,0:T(2,128)(2,1)}, u32[]{:S(2)}) copy-start(bf16[1,512]{1,0:T(2,128)(2,1)} %get-tuple-element.76) | copy-start | bytes 3076
  168.3 40.5 %copy-start.31 = (f32[1,8,15,31]{3,1,2,0:T(8,128)S(1)}, f32[1,8,15,31]{3,1,2,0:T(8,128)}, u32[]{:S(2)}) copy-start(f32[1,8,15,31]{3,1,2,0:T(8,128)} %get-tuple-element.72) | copy-start | bytes 44644
  168.4 40.5 %copy-start.39 = (s32[6,8]{1,0:T(8,128)S(1)}, s32[6,8]{1,0:T(8,128)}, u32[]{:S(2)}) copy-start(s32[6,8]{1,0:T(8,128)} %copy-done.38) | copy-start | bytes 580
  168.4 65.4 %all-gather.11.cloned.1.call-start = ((), (), s32[]{:S(2)}) async-start(), calls=%async_computation.2 | async-start | bytes 1966080 | tf_op jit(solution)/shard_map/all_gather | solution.py:68
  202.9 177.3 %all-gather.13.cloned.1.call-start = ((), (), s32[]{:S(2)}) async-start(), calls=%async_computation.3 | async-start | bytes 1966080 | tf_op jit(solution)/shard_map/all_gather | solution.py:127
  209.1 6.4 %copy-start.33 = (s32[16,32]{1,0:T(8,128)S(1)}, s32[16,32]{1,0:T(8,128)}, u32[]{:S(2)}) copy-start(s32[16,32]{1,0:T(8,128)} %copy-done.32) | copy-start | bytes 6148
  212.3 6.3 %copy-start.36 = (s32[16,32]{1,0:T(8,128)S(1)}, s32[16,32]{1,0:T(8,128)}, u32[]{:S(2)}) copy-start(s32[16,32]{1,0:T(8,128)} %copy-done.35) | copy-start | bytes 6148
  235.6 3.2 copy-start.5
  235.6 3.3 copy-start.49
  241.5 0.8 copy-start.1
  243.4 13.5 %collective-permute-start.2 = (bf16[256,1024]{1,0:T(8,128)(2,1)}, bf16[256,1024]{1,0:T(8,128)(2,1)}, u32[]{:S(2)}, u32[]{:S(2)}) collective-permute-start(bf16[256,1024]{1,0:T(8,128)(2,1)} %get-tuple-element.63), channel_id=1, source_target_pairs={{0,4},{4,8},{8,12},{12,16},{16,20},{20,24},{24,28},{1,5},{5,9},{9,... | collective-permute-start | bytes 1572872 | tf_op jit(solution)/shard_map/ppermute | solution.py:23
  247.2 10.8 %collective-permute-start.3 = (bf16[256,1024]{1,0:T(8,128)(2,1)}, bf16[256,1024]{1,0:T(8,128)(2,1)}, u32[]{:S(2)}, u32[]{:S(2)}) collective-permute-start(bf16[256,1024]{1,0:T(8,128)(2,1)} %get-tuple-element.64), channel_id=1, source_target_pairs={{4,0},{8,4},{12,8},{16,12},{20,16},{24,20},{28,24},{5,1},{9,5},{13... | collective-permute-start | bytes 1572872 | tf_op jit(solution)/shard_map/ppermute | solution.py:24
  274.5 27.9 %copy-start.17 = (bf16[6,16,8,64]{3,2,1,0:T(8,128)(2,1)S(1)}, bf16[6,16,8,64]{3,2,1,0:T(8,128)(2,1)}, u32[]{:S(2)}) copy-start(bf16[6,16,8,64]{3,2,1,0:T(8,128)(2,1)} %get-tuple-element.59) | copy-start | bytes 294916
  274.5 27.9 %copy-start.45 = (pred[16,32]{1,0:T(8,128)(4,1)S(1)}, pred[16,32]{1,0:T(8,128)(4,1)}, u32[]{:S(2)}) copy-start(pred[16,32]{1,0:T(8,128)(4,1)} %fusion.392) | copy-start | bytes 1540
  310.3 4.3 copy-start.14
  322.4 4.3 copy-start.11
  334.9 4.3 copy-start.8
  346.1 3.7 copy-start.23
  346.1 3.7 copy-start.26
  346.1 3.7 copy-start.29
  346.1 34.1 %copy-start.20 = (bf16[384,512]{1,0:T(8,128)(2,1)S(1)}, bf16[384,512]{1,0:T(8,128)(2,1)}, u32[]{:S(2)}) copy-start(bf16[384,512]{1,0:T(8,128)(2,1)} %fusion.204) | copy-start | bytes 1179652
  350.6 33.5 %copy-start.50 = (bf16[1,512]{1,0:T(2,128)(2,1)S(1)}, bf16[1,512]{1,0:T(2,128)(2,1)}, u32[]{:S(2)}) copy-start(bf16[1,512]{1,0:T(2,128)(2,1)} %get-tuple-element.74) | copy-start | bytes 3076
  350.7 39.4 %copy-start.30 = (f32[1,8,15,31]{3,1,2,0:T(8,128)S(1)}, f32[1,8,15,31]{3,1,2,0:T(8,128)}, u32[]{:S(2)}) copy-start(f32[1,8,15,31]{3,1,2,0:T(8,128)} %get-tuple-element.71) | copy-start | bytes 44644
  350.7 39.3 %copy-start.40 = (s32[6,8]{1,0:T(8,128)S(1)}, s32[6,8]{1,0:T(8,128)}, u32[]{:S(2)}) copy-start(s32[6,8]{1,0:T(8,128)} %copy-done.38) | copy-start | bytes 580
  350.7 64.3 %all-gather.15.cloned.1.call-start = ((), (), s32[]{:S(2)}) async-start(), calls=%async_computation.4 | async-start | bytes 1966080 | tf_op jit(solution)/shard_map/all_gather | solution.py:68
  384.1 177.2 %all-gather.17.cloned.1.call-start = ((), (), s32[]{:S(2)}) async-start(), calls=%async_computation.5 | async-start | bytes 1966080 | tf_op jit(solution)/shard_map/all_gather | solution.py:127
  390.3 6.4 %copy-start.34 = (s32[16,32]{1,0:T(8,128)S(1)}, s32[16,32]{1,0:T(8,128)}, u32[]{:S(2)}) copy-start(s32[16,32]{1,0:T(8,128)} %copy-done.32) | copy-start | bytes 6148
  393.5 6.3 %copy-start.37 = (s32[16,32]{1,0:T(8,128)S(1)}, s32[16,32]{1,0:T(8,128)}, u32[]{:S(2)}) copy-start(s32[16,32]{1,0:T(8,128)} %copy-done.35) | copy-start | bytes 6148
  399.8 17.0 %copy-start.48 = (f32[1,2048]{1,0:T(1,128)S(1)}, f32[1,2048]{1,0:T(1,128)}, u32[]{:S(2)}) copy-start(f32[1,2048]{1,0:T(1,128)} %mul.147) | copy-start | bytes 24580
  416.8 3.2 copy-start.4
  422.6 0.8 copy-start.2
  424.6 13.5 %collective-permute-start.4 = (bf16[256,1024]{1,0:T(8,128)(2,1)}, bf16[256,1024]{1,0:T(8,128)(2,1)}, u32[]{:S(2)}, u32[]{:S(2)}) collective-permute-start(bf16[256,1024]{1,0:T(8,128)(2,1)} %get-tuple-element.57), channel_id=1, source_target_pairs={{0,4},{4,8},{8,12},{12,16},{16,20},{20,24},{24,28},{1,5},{5,9},{9,... | collective-permute-start | bytes 1572872 | tf_op jit(solution)/shard_map/ppermute | solution.py:23
  428.4 10.8 %collective-permute-start.5 = (bf16[256,1024]{1,0:T(8,128)(2,1)}, bf16[256,1024]{1,0:T(8,128)(2,1)}, u32[]{:S(2)}, u32[]{:S(2)}) collective-permute-start(bf16[256,1024]{1,0:T(8,128)(2,1)} %get-tuple-element.58), channel_id=1, source_target_pairs={{4,0},{8,4},{12,8},{16,12},{20,16},{24,20},{28,24},{5,1},{9,5},{13... | collective-permute-start | bytes 1572872 | tf_op jit(solution)/shard_map/ppermute | solution.py:24
  455.7 27.9 %copy-start.15 = (bf16[6,16,8,64]{3,2,1,0:T(8,128)(2,1)S(1)}, bf16[6,16,8,64]{3,2,1,0:T(8,128)(2,1)}, u32[]{:S(2)}) copy-start(bf16[6,16,8,64]{3,2,1,0:T(8,128)(2,1)} %get-tuple-element.53) | copy-start | bytes 294916
  455.7 27.9 %copy-start.46 = (pred[16,32]{1,0:T(8,128)(4,1)S(1)}, pred[16,32]{1,0:T(8,128)(4,1)}, u32[]{:S(2)}) copy-start(pred[16,32]{1,0:T(8,128)(4,1)} %fusion.392) | copy-start | bytes 1540
  491.5 4.3 copy-start.12
  491.5 4.3 copy-start.43
  503.6 4.3 copy-start.9
  503.6 4.3 copy-start.42
  515.9 4.3 copy-start.6
  516.0 4.3 copy-start.41
  527.1 3.7 copy-start.21
  527.1 3.7 copy-start.24
  527.1 3.7 copy-start.27
  527.2 34.1 %copy-start.19 = (bf16[384,512]{1,0:T(8,128)(2,1)S(1)}, bf16[384,512]{1,0:T(8,128)(2,1)}, u32[]{:S(2)}) copy-start(bf16[384,512]{1,0:T(8,128)(2,1)} %fusion.201) | copy-start | bytes 1179652
Sparse Core Ops, SparseCore 0:
  9.2 31.7 all-gather.6
  168.5 30.5 all-gather.8
  203.0 30.7 all-gather.10
  350.8 29.3 all-gather.12
  384.2 30.7 all-gather.14
  531.8 29.3 all-gather.16
where the time goes:
time: 580 us; the launch traced here: 572 us
  matrix products  197 us (34%)
  local copies, waits for them, and re-layouts  152 us (26%)
  waiting for transfers between devices  129 us (22%)
  other arithmetic  32.9 us (6%)
  starting transfers between devices  29.4 us (5%)
  blocking collectives  16.6 us (3%)
  between operations  14.8 us (3%)
    all_gather x3, waiting for transfers between devices, per_device(): lax.all_gather(part, 'tp', axis=1, tiled=True)  89.6 us
    dot_general x12, matrix products, one_row(): jnp.einsum('whd,rshd->hwrs', query_tile, slab_keys, preferred_element_typ...  83.6 us
    gather x54, local copies, waits for them, and re-layouts  83.1 us
    dot_general x12, matrix products, one_row(): jnp.einsum('hwrs,rshd->whd', weights, slab_values, preferred_element_type...  40.8 us
    dot_general x12, matrix products, contract(): lax.dot_general(left, right, (((1,), (1,)), ((), ())), preferred_element_...  39.1 us
    all_gather x3, waiting for transfers between devices, per_device(): lax.all_gather(stream, 'tp', axis=1, tiled=True)  36.5 us
    dot_general x12, matrix products, one_row(): jnp.einsum('hrb,wsb->hwrs', row_bias, onehot, precision=lax.Precision.HIG...  32.9 us
    unnamed x107, local copies, waits for them, and re-layouts  25.7 us
  transfers between devices with their start and end apart: 12, of which 8 were waited for; matrix products, arithmetic and copies ran while one was open for 11% of the time, Pallas kernels for 0%

commit v1 on v0

--- a/solution.py
+++ b/solution.py
@@ -1,6 +1,8 @@
 import jax
 import jax.numpy as jnp
 from jax import lax
+from jax.experimental import pallas as pl
+from jax.experimental.pallas import tpu as pltpu
 from jax.sharding import PartitionSpec as P
 
 HEAD_DIM = 64
@@ -36,7 +38,7 @@
     )
 
 
-def per_device(residual, norm_gain, w_query, w_key, w_value, w_out, offset_bias):
+def generic_device(residual, norm_gain, w_query, w_key, w_value, w_out, offset_bias):
     token_count = residual.shape[0]
     local_feats = residual.shape[1]
     local_heads = offset_bias.shape[1]
@@ -132,6 +134,115 @@
     return stream
 
 
+def bias_lanes(offset_bias):
+    layers, heads, row_offs, col_offs = offset_bias.shape
+    flipped = jnp.flip(offset_bias, axis=3)
+    padded = jnp.pad(flipped, ((0, 0), (0, 0), (0, 1), (0, GRID_W - col_offs)))
+    paired = padded.reshape(layers, heads // 2, 2, row_offs + 1, GRID_W)
+    return paired.transpose(0, 1, 3, 2, 4).reshape(layers, heads // 2, row_offs + 1, 2 * GRID_W)
+
+
+def window_mask():
+    shape = (GRID_W, 2 * GRID_W)
+    key_col = lax.broadcasted_iota(jnp.int32, shape, 0)
+    query_col = lax.broadcasted_iota(jnp.int32, shape, 1) % GRID_W
+    first = jnp.clip(query_col - NA_COLS // 2, 0, GRID_W - NA_COLS)
+    return (key_col >= first) & (key_col < first + NA_COLS)
+
+
+def build_table(lanes_of, table):
+    inside = window_mask()
+    for off in range(2 * NA_ROWS - 1):
+        row = jnp.broadcast_to(lanes_of(off), (GRID_W, 2 * GRID_W))
+        rolled = pltpu.roll(row, 2 * GRID_W - (NA_COLS - 1), axis=1, stride=1, stride_axis=0)
+        table[off * GRID_W : (off + 1) * GRID_W, :] = jnp.where(inside, rolled, -1e30)
+
+
+def attend_row(query, window_keys, window_values, bias):
+    low = lax.broadcasted_iota(jnp.int32, query.shape, 1) < HEAD_DIM
+    zero = jnp.zeros_like(query)
+    block = jnp.concatenate([jnp.where(low, query, zero), jnp.where(low, zero, query)], axis=0)
+    scores = contract(window_keys, block) + bias
+    top = jnp.max(scores, axis=0, keepdims=True)
+    weights = jnp.exp(scores - top)
+    inverse = 1.0 / jnp.sum(weights, axis=0, keepdims=True)
+    weights = (weights * inverse).astype(jnp.bfloat16)
+    mixed = lax.dot_general(
+        weights, window_values, (((0,), (0,)), ((), ())), preferred_element_type=jnp.float32
+    )
+    return jnp.where(low, mixed[:GRID_W], mixed[GRID_W:]).astype(jnp.bfloat16)
+
+
+def row_window(row, rows_dev, rows_all):
+    reach = NA_ROWS // 2
+    row_base = lax.axis_index("sp") * rows_dev
+    first = jnp.clip(row_base + row - reach, 0, rows_all - NA_ROWS)
+    return first - row_base + reach, first - row_base - row + NA_ROWS - 1
+
+
+def attention_kernel(rows_dev, rows_all, q_ref, kv_ref, lanes_ref, out_ref, table):
+    width = q_ref.shape[1]
+    for pair in range(width // 128):
+        build_table(lambda off: lanes_ref[pair, off : off + 1, :], table)
+        cols = slice(pair * 128, (pair + 1) * 128)
+        vcols = slice(width + pair * 128, width + (pair + 1) * 128)
+
+        def one_row(row, carry):
+            start, off = row_window(row, rows_dev, rows_all)
+            keys = pl.ds(pl.multiple_of(start * GRID_W, GRID_W), NA_ROWS * GRID_W)
+            here = pl.ds(pl.multiple_of(row * GRID_W, GRID_W), GRID_W)
+            bias = table[pl.ds(pl.multiple_of(off * GRID_W, GRID_W), NA_ROWS * GRID_W), :]
+            out_ref[here, cols] = attend_row(
+                q_ref[here, cols], kv_ref[keys, cols], kv_ref[keys, vcols], bias
+            )
+            return carry
+
+        lax.fori_loop(0, rows_dev, one_row, 0)
+
+
+def attention(queries, padded, lanes, rows_dev, rows_all):
+    vmem = pl.BlockSpec(memory_space=pltpu.VMEM)
+    return pl.pallas_call(
+        lambda *refs: attention_kernel(rows_dev, rows_all, *refs),
+        out_shape=jax.ShapeDtypeStruct(queries.shape, jnp.bfloat16),
+        in_specs=[vmem] * 3,
+        out_specs=vmem,
+        scratch_shapes=[pltpu.VMEM(((2 * NA_ROWS - 1) * GRID_W, 2 * GRID_W), jnp.float32)],
+        name="attention",
+    )(queries, padded, lanes)
+
+
+def paired_device(residual, norm_gain, w_query, w_key, w_value, w_out, offset_bias):
+    token_count = residual.shape[0]
+    rows_dev = token_count // GRID_W
+    rows_all = rows_dev * lax.axis_size("sp")
+    reach = NA_ROWS // 2
+    lanes = bias_lanes(offset_bias)
+    gains = lax.all_gather(norm_gain, "tp", axis=1, tiled=True).astype(jnp.float32)
+    stream = residual
+    for layer_index in range(LAYERS):
+        full_float = lax.all_gather(stream, "tp", axis=1, tiled=True).astype(jnp.float32)
+        inverse = lax.rsqrt(jnp.mean(full_float * full_float, axis=1, keepdims=True) + epsilon)
+        normed = (full_float * inverse * gains[layer_index][None, :]).astype(jnp.bfloat16)
+        keys = contract(normed, w_key[layer_index]).astype(jnp.bfloat16)
+        values = contract(normed, w_value[layer_index]).astype(jnp.bfloat16)
+        key_value = jnp.concatenate([keys, values], axis=1)
+        padded = padded_2(key_value, (("sp", 0),), reach * GRID_W)
+        queries = contract(normed, w_query[layer_index]).astype(jnp.bfloat16)
+        queries = queries * jnp.bfloat16(HEAD_DIM ** (-0.5))
+        attended = attention(queries, padded, lanes[layer_index], rows_dev, rows_all)
+        gathered = lax.all_gather(attended, "tp", axis=1, tiled=True)
+        mixed = contract(gathered, w_out[layer_index])
+        stream = (stream.astype(jnp.float32) + mixed).astype(jnp.bfloat16)
+    return stream
+
+
+def per_device(residual, norm_gain, w_query, w_key, w_value, w_out, offset_bias):
+    fits = offset_bias.shape[1] % 2 == 0 and 2 * HEAD_DIM == 128 and 2 * GRID_W == 128
+    body = paired_device if fits else generic_device
+    return body(residual, norm_gain, w_query, w_key, w_value, w_out, offset_bias)
+
+
 def solution(mesh):
     in_specs = (
         P("sp", "tp"),

time: 580 us -> 338 us (0.58)
  matrix products: 197 us -> 39.1 us
  local copies, waits for them, and re-layouts: 152 us -> 3.31 us
  waiting for transfers between devices: 129 us -> 190 us
  Pallas kernels: 0 us -> 49.2 us
  other arithmetic: 32.9 us -> 15.9 us
  starting transfers between devices: 29.4 us -> 17.6 us
  blocking collectives: 16.6 us -> 6.17 us
    dot_general x39 -> x0, matrix products: 158 us -> none  [the longest x12 83.6 us: one_row(): jnp.einsum('whd,rshd->hwrs', query_tile, slab_keys, preferred_element_typ...]
    gather x54 -> x0, local copies, waits for them, and re-layouts: 83.1 us -> none
    all_gather x6, waiting for transfers between devices: 126 us -> 175 us  [the longest x3 87.8 us: paired_device(): lax.all_gather(stream, 'tp', axis=1, tiled=True).astype(jnp.float32)]
    pallas_call x0 -> x3, Pallas kernels: none -> 49.2 us  [attention(): pl.pallas_call(lambda *refs: attention_kernel(rows_dev, rows_all, *refs),...]
    reshape x18 -> x1, local copies, waits for them, and re-layouts: 32.6 us -> 0.09 us  [bias_lanes(): paired = padded.reshape(layers, heads // 2, 2, row_offs + 1, GRID_W)]
    unnamed x107 -> x14, local copies, waits for them, and re-layouts: 25.7 us -> 0.03 us
    ppermute x3, starting transfers between devices: 17.7 us -> 5.95 us  [padded_2(): after = lax.ppermute(first, axis, down)]
    ppermute x3, waiting for transfers between devices: 2.24 us -> 12.8 us  [padded_2(): after = lax.ppermute(first, axis, down)]
  transfers between devices with their start and end apart: 12 -> 12, of which waited for: 8 -> 12; matrix products, arithmetic and copies ran while one was open for 11% -> 4% of each run, Pallas kernels for 0% -> 0%
where the time goes in v1:
time: 338 us; the launch traced here: 335 us
  waiting for transfers between devices  190 us (56%)
  Pallas kernels  49.2 us (15%)
  matrix products  39.1 us (12%)
  starting transfers between devices  17.6 us (5%)
  other arithmetic  15.9 us (5%)
  between operations  13.7 us (4%)
  blocking collectives  6.17 us (2%)
    all_gather x3, waiting for transfers between devices, paired_device(): lax.all_gather(stream, 'tp', axis=1, tiled=True).astype(jnp.float32)  87.8 us
    all_gather x3, waiting for transfers between devices, paired_device(): gathered = lax.all_gather(attended, 'tp', axis=1, tiled=True)  87.7 us
    pallas_call x3, Pallas kernels, attention(): pl.pallas_call(lambda *refs: attention_kernel(rows_dev, rows_all, *refs),...  49.2 us
    dot_general x12, matrix products, contract(): lax.dot_general(left, right, (((1,), (1,)), ((), ())), preferred_element_...  39.1 us
    ppermute x3, waiting for transfers between devices, padded_2(): after = lax.ppermute(first, axis, down)  12.8 us
    ppermute x3, starting transfers between devices, padded_2(): before = lax.ppermute(last, axis, up)  11.5 us
    concatenate x3, other arithmetic, padded_2(): array = jnp.concatenate([before, array, after], axis=dim)  7.46 us
  transfers between devices with their start and end apart: 12, of which 12 were waited for; matrix products, arithmetic and copies ran while one was open for 4% of the time, Pallas kernels for 0%

profile of v1, /device:TPU:11, one launch (start us, length us, event | category | flops | bytes accessed | tf_op | source)
XLA Modules:
  0.0 335.0 jit_solution(10242234918923697096)
XLA Ops:
  6.5 0.0 all-gather.7.cloned.1.call-start
  6.5 0.7 all-gather.7.cloned.1.call-update
  7.3 0.0 all-gather.9.cloned.1.call-start
  7.3 1.0 rev.4
  8.4 0.1 copy.10
  8.5 6.2 %all_gather.22 = bf16[3,2048]{1,0:T(4,128)(2,1)S(1)} all-gather(bf16[3,512]{1,0:T(4,128)(2,1)} %param.8), channel_id=1, replica_groups=mesh['sp'=8,'tp'=4] {'tp'}, dimensions={1}, use_global_device_ids=true | all-gather | bytes 15360 | tf_op jit(solution)/shard_map/all_gather | solution.py:221
  14.6 26.2 %all-gather.7.cloned.1.call-done = bf16[384,2048]{1,0:T(8,128)(2,1)} async-done(((bf16[384,512]{1,0:T(8,128)(2,1)}), bf16[384,2048]{1,0:T(8,128)(2,1)}) %all-gather.7.cloned.1.call-update) | async-done | bytes 1572880 | tf_op jit(solution)/shard_map/all_gather | solution.py:224
  40.9 1.8 fusion
  42.7 3.2 fusion.66
  45.9 0.0 copy-done
  45.9 2.6 fusion.69
  48.5 1.2 fusion.101
  49.7 3.8 %collective-permute-start = (bf16[256,1024]{1,0:T(8,128)(2,1)}, bf16[256,1024]{1,0:T(8,128)(2,1)S(1)}, u32[]{:S(2)}, u32[]{:S(2)}) collective-permute-start(bf16[256,1024]{1,0:T(8,128)(2,1)} %get-tuple-element.9), channel_id=1, source_target_pairs={{0,4},{4,8},{8,12},{12,16},{16,20},{20,24},{24,28},{1,5},{5,9},{9,... | collective-permute-start | bytes 1572872 | tf_op jit(solution)/shard_map/ppermute | solution.py:25
  53.5 1.9 collective-permute-start.1
  55.5 0.7 squeeze.48.refs_2_
  56.2 3.4 %fusion.96.refs_0_ = bf16[384,512]{1,0:T(8,128)(2,1)} fusion(bf16[3,512,2048]{2,1,0:T(8,128)(2,1)} %param.9, bf16[384,2048]{1,0:T(8,128)(2,1)S(1)} %copy-done, f32[2048]{0:T(1024)S(1)} %bitcast.92, f32[384]{0:T(512)S(1)} %add_rsqrt_fusion.2), kind=kOutput, calls=%fused_computation.71 | convolution fusion | flops 808845312 | bytes 4072960 | tf_op jit(solution)/shard_map/dot_general | solution.py:36
  59.6 0.4 collective-permute-done
  59.9 4.4 %collective-permute-done.1 = bf16[256,1024]{1,0:T(8,128)(2,1)} collective-permute-done((bf16[256,1024]{1,0:T(8,128)(2,1)}, bf16[256,1024]{1,0:T(8,128)(2,1)}, u32[]{:S(2)}, u32[]{:S(2)}) %collective-permute-start.1) | collective-permute-done | bytes 524320 | tf_op jit(solution)/shard_map/ppermute | solution.py:26
  64.3 2.5 pad_maximum_fusion.refs_1_
  66.8 16.4 %attention.3 = bf16[384,512]{1,0:T(8,128)(2,1)} custom-call(bf16[384,512]{1,0:T(8,128)(2,1)} %fusion.96.refs_0_, bf16[896,1024]{1,0:T(8,128)(2,1)} %pad_maximum_fusion.refs_1_, f32[4,16,128]{2,1,0:T(8,128)} %squeeze.48.refs_2_), custom_call_target="tpu_custom_call" | custom-call | tf_op jit(solution)/shard_map/attention/pallas_call | solution.py:205
  83.2 0.0 all-gather.9.cloned.1.call-update
  83.2 0.0 all-gather.11.cloned.1.call-start
  83.3 29.2 %all-gather.9.cloned.1.call-done = bf16[384,2048]{1,0:T(8,128)(2,1)} async-done(((bf16[384,512]{1,0:T(8,128)(2,1)}), bf16[384,2048]{1,0:T(8,128)(2,1)}) %all-gather.9.cloned.1.call-update) | async-done | bytes 1572880 | tf_op jit(solution)/shard_map/all_gather | solution.py:234
  112.5 0.0 copy-done.3
  112.5 3.8 %fusion.60 = bf16[384,512]{1,0:T(8,128)(2,1)} fusion(bf16[384,2048]{1,0:T(8,128)(2,1)} %all-gather.9.cloned.1.call-done, bf16[3,512,2048]{2,1,0:T(8,128)(2,1)} %param.12, bf16[384,512]{1,0:T(8,128)(2,1)S(1)} %copy-done.3), kind=kOutput, calls=%fused_computation.59 | convolution fusion | flops 805896192 | bytes 4456448 | tf_op jit(solution)/shard_map/dot_general | solution.py:36
  116.3 0.0 all-gather.11.cloned.1.call-update
  116.3 0.0 all-gather.13.cloned.1.call-start
  116.4 30.8 %all-gather.11.cloned.1.call-done = bf16[384,2048]{1,0:T(8,128)(2,1)} async-done(((bf16[384,512]{1,0:T(8,128)(2,1)}), bf16[384,2048]{1,0:T(8,128)(2,1)}) %all-gather.11.cloned.1.call-update) | async-done | bytes 1572880 | tf_op jit(solution)/shard_map/all_gather | solution.py:224
  147.2 1.8 fusion.3
  149.0 0.0 copy-start.2
  149.0 3.2 fusion.75
  152.2 0.0 copy-done.2
  152.2 2.6 fusion.78
  154.9 0.9 fusion.100
  155.8 3.8 %collective-permute-start.2 = (bf16[256,1024]{1,0:T(8,128)(2,1)}, bf16[256,1024]{1,0:T(8,128)(2,1)S(1)}, u32[]{:S(2)}, u32[]{:S(2)}) collective-permute-start(bf16[256,1024]{1,0:T(8,128)(2,1)} %get-tuple-element.7), channel_id=1, source_target_pairs={{0,4},{4,8},{8,12},{12,16},{16,20},{20,24},{24,28},{1,5},{5,9},{9,... | collective-permute-start | bytes 1572872 | tf_op jit(solution)/shard_map/ppermute | solution.py:25
  159.7 2.1 collective-permute-start.3
  161.8 0.7 squeeze.53.refs_2_
  162.5 3.4 %fusion.93.refs_0_ = bf16[384,512]{1,0:T(8,128)(2,1)} fusion(bf16[3,512,2048]{2,1,0:T(8,128)(2,1)} %param.9, bf16[384,2048]{1,0:T(8,128)(2,1)S(1)} %copy-done.2, f32[2048]{0:T(1024)S(1)} %bitcast.89, f32[384]{0:T(512)} %copy-done.6), kind=kOutput, calls=%fused_computation.70 | convolution fusion | flops 808845312 | bytes 4073472 | tf_op jit(solution)/shard_map/dot_general | solution.py:36
  165.9 0.2 collective-permute-done.2
  166.1 4.2 %collective-permute-done.3 = bf16[256,1024]{1,0:T(8,128)(2,1)} collective-permute-done((bf16[256,1024]{1,0:T(8,128)(2,1)S(1)}, bf16[256,1024]{1,0:T(8,128)(2,1)}, u32[]{:S(2)}, u32[]{:S(2)}) %collective-permute-start.3) | collective-permute-done | bytes 524320 | tf_op jit(solution)/shard_map/ppermute | solution.py:26
  170.3 2.5 pad_maximum_fusion.1.refs_1_
  172.7 16.4 %attention.4 = bf16[384,512]{1,0:T(8,128)(2,1)} custom-call(bf16[384,512]{1,0:T(8,128)(2,1)} %fusion.93.refs_0_, bf16[896,1024]{1,0:T(8,128)(2,1)} %pad_maximum_fusion.1.refs_1_, f32[4,16,128]{2,1,0:T(8,128)} %squeeze.53.refs_2_), custom_call_target="tpu_custom_call" | custom-call | tf_op jit(solution)/shard_map/attention/pallas_call | solution.py:205
  189.1 0.0 all-gather.13.cloned.1.call-update
  189.2 0.0 all-gather.15.cloned.1.call-start
  189.2 29.2 %all-gather.13.cloned.1.call-done = bf16[384,2048]{1,0:T(8,128)(2,1)} async-done(((bf16[384,512]{1,0:T(8,128)(2,1)}), bf16[384,2048]{1,0:T(8,128)(2,1)}) %all-gather.13.cloned.1.call-update) | async-done | bytes 1572880 | tf_op jit(solution)/shard_map/all_gather | solution.py:234
  218.4 3.8 %fusion.57 = bf16[384,512]{1,0:T(8,128)(2,1)} fusion(bf16[384,2048]{1,0:T(8,128)(2,1)} %all-gather.13.cloned.1.call-done, bf16[3,512,2048]{2,1,0:T(8,128)(2,1)} %param.12, bf16[384,512]{1,0:T(8,128)(2,1)S(1)} %copy-done.5), kind=kOutput, calls=%fused_computation.58 | convolution fusion | flops 805896192 | bytes 4456448 | tf_op jit(solution)/shard_map/dot_general | solution.py:36
  222.3 0.0 all-gather.15.cloned.1.call-update
  222.3 0.0 all-gather.17.cloned.1.call-start
  222.3 30.8 %all-gather.15.cloned.1.call-done = bf16[384,2048]{1,0:T(8,128)(2,1)} async-done(((bf16[384,512]{1,0:T(8,128)(2,1)}), bf16[384,2048]{1,0:T(8,128)(2,1)}) %all-gather.15.cloned.1.call-update) | async-done | bytes 1572880 | tf_op jit(solution)/shard_map/all_gather | solution.py:224
  253.1 1.8 fusion.6
  254.9 3.2 fusion.84
  258.2 2.6 fusion.87
  260.8 0.9 fusion.99
  261.7 3.8 %collective-permute-start.4 = (bf16[256,1024]{1,0:T(8,128)(2,1)}, bf16[256,1024]{1,0:T(8,128)(2,1)S(1)}, u32[]{:S(2)}, u32[]{:S(2)}) collective-permute-start(bf16[256,1024]{1,0:T(8,128)(2,1)} %get-tuple-element.5), channel_id=1, source_target_pairs={{0,4},{4,8},{8,12},{12,16},{16,20},{20,24},{24,28},{1,5},{5,9},{9,... | collective-permute-start | bytes 1572872 | tf_op jit(solution)/shard_map/ppermute | solution.py:25
  265.6 1.9 collective-permute-start.5
  267.5 0.7 squeeze.58.refs_2_
  268.2 3.4 %fusion.90.refs_0_ = bf16[384,512]{1,0:T(8,128)(2,1)} fusion(bf16[3,512,2048]{2,1,0:T(8,128)(2,1)} %param.9, bf16[384,2048]{1,0:T(8,128)(2,1)S(1)} %copy-done.1, f32[2048]{0:T(1024)S(1)} %bitcast.86, f32[384]{0:T(512)S(1)} %add_rsqrt_fusion), kind=kOutput, calls=%fused_computation.69 | convolution fusion | flops 808845312 | bytes 4072960 | tf_op jit(solution)/shard_map/dot_general | solution.py:36
  271.6 0.4 collective-permute-done.4
  272.0 4.2 %collective-permute-done.5 = bf16[256,1024]{1,0:T(8,128)(2,1)} collective-permute-done((bf16[256,1024]{1,0:T(8,128)(2,1)S(1)}, bf16[256,1024]{1,0:T(8,128)(2,1)}, u32[]{:S(2)}, u32[]{:S(2)}) %collective-permute-start.5) | collective-permute-done | bytes 524320 | tf_op jit(solution)/shard_map/ppermute | solution.py:26
  276.2 2.5 pad_maximum_fusion.2.refs_1_
  278.7 16.4 %attention.5 = bf16[384,512]{1,0:T(8,128)(2,1)} custom-call(bf16[384,512]{1,0:T(8,128)(2,1)} %fusion.90.refs_0_, bf16[896,1024]{1,0:T(8,128)(2,1)} %pad_maximum_fusion.2.refs_1_, f32[4,16,128]{2,1,0:T(8,128)} %squeeze.58.refs_2_), custom_call_target="tpu_custom_call" | custom-call | tf_op jit(solution)/shard_map/attention/pallas_call | solution.py:205
  295.1 0.0 all-gather.17.cloned.1.call-update
  295.1 29.3 %all-gather.17.cloned.1.call-done = bf16[384,2048]{1,0:T(8,128)(2,1)} async-done(((bf16[384,512]{1,0:T(8,128)(2,1)}), bf16[384,2048]{1,0:T(8,128)(2,1)}) %all-gather.17.cloned.1.call-update) | async-done | bytes 1572880 | tf_op jit(solution)/shard_map/all_gather | solution.py:234
  324.3 3.8 %fusion.54 = bf16[384,512]{1,0:T(8,128)(2,1)} fusion(bf16[384,2048]{1,0:T(8,128)(2,1)} %all-gather.17.cloned.1.call-done, bf16[3,512,2048]{2,1,0:T(8,128)(2,1)} %param.12, bf16[384,512]{1,0:T(8,128)(2,1)S(1)} %copy-done.4), kind=kOutput, calls=%fused_computation.57 | convolution fusion | flops 805896192 | bytes 4456448 | tf_op jit(solution)/shard_map/dot_general | solution.py:36
  (16 shorter events, 0.1 us)
Async XLA Ops:
  6.5 34.3 %all-gather.7.cloned.1.call-start = ((), (), s32[]{:S(2)}) async-start(), calls=%async_computation | async-start | bytes 1966080 | tf_op jit(solution)/shard_map/all_gather | solution.py:224
  7.3 105.2 %all-gather.9.cloned.1.call-start = ((), (), s32[]{:S(2)}) async-start(), calls=%async_computation.1 | async-start | bytes 1966080 | tf_op jit(solution)/shard_map/all_gather | solution.py:234
  42.7 3.2 copy-start
  49.7 10.3 %collective-permute-start = (bf16[256,1024]{1,0:T(8,128)(2,1)}, bf16[256,1024]{1,0:T(8,128)(2,1)S(1)}, u32[]{:S(2)}, u32[]{:S(2)}) collective-permute-start(bf16[256,1024]{1,0:T(8,128)(2,1)} %get-tuple-element.9), channel_id=1, source_target_pairs={{0,4},{4,8},{8,12},{12,16},{16,20},{20,24},{24,28},{1,5},{5,9},{9,... | collective-permute-start | bytes 1572872 | tf_op jit(solution)/shard_map/ppermute | solution.py:25
  53.5 10.8 %collective-permute-start.1 = (bf16[256,1024]{1,0:T(8,128)(2,1)}, bf16[256,1024]{1,0:T(8,128)(2,1)}, u32[]{:S(2)}, u32[]{:S(2)}) collective-permute-start(bf16[256,1024]{1,0:T(8,128)(2,1)} %get-tuple-element.10), channel_id=1, source_target_pairs={{4,0},{8,4},{12,8},{16,12},{20,16},{24,20},{28,24},{5,1},{9,5},{13... | collective-permute-start | bytes 1572872 | tf_op jit(solution)/shard_map/ppermute | solution.py:26
  59.5 52.9 %copy-start.3 = (bf16[384,512]{1,0:T(8,128)(2,1)S(1)}, bf16[384,512]{1,0:T(8,128)(2,1)}, u32[]{:S(2)}) copy-start(bf16[384,512]{1,0:T(8,128)(2,1)} %param.7) | copy-start | bytes 1179652
  83.2 64.0 %all-gather.11.cloned.1.call-start = ((), (), s32[]{:S(2)}) async-start(), calls=%async_computation.2 | async-start | bytes 1966080 | tf_op jit(solution)/shard_map/all_gather | solution.py:224
  116.3 102.1 %all-gather.13.cloned.1.call-start = ((), (), s32[]{:S(2)}) async-start(), calls=%async_computation.3 | async-start | bytes 1966080 | tf_op jit(solution)/shard_map/all_gather | solution.py:234
  149.0 6.8 %copy-start.6 = (f32[384]{0:T(512)}, f32[384]{0:T(512)S(1)}, u32[]{:S(2)}) copy-start(f32[384]{0:T(512)S(1)} %add_rsqrt_fusion.1) | copy-start | bytes 4612
  149.0 3.2 copy-start.2
  155.8 10.3 %collective-permute-start.2 = (bf16[256,1024]{1,0:T(8,128)(2,1)}, bf16[256,1024]{1,0:T(8,128)(2,1)S(1)}, u32[]{:S(2)}, u32[]{:S(2)}) collective-permute-start(bf16[256,1024]{1,0:T(8,128)(2,1)} %get-tuple-element.7), channel_id=1, source_target_pairs={{0,4},{4,8},{8,12},{12,16},{16,20},{20,24},{24,28},{1,5},{5,9},{9,... | collective-permute-start | bytes 1572872 | tf_op jit(solution)/shard_map/ppermute | solution.py:25
  159.7 10.6 %collective-permute-start.3 = (bf16[256,1024]{1,0:T(8,128)(2,1)S(1)}, bf16[256,1024]{1,0:T(8,128)(2,1)}, u32[]{:S(2)}, u32[]{:S(2)}) collective-permute-start(bf16[256,1024]{1,0:T(8,128)(2,1)S(1)} %get-tuple-element.8), channel_id=1, source_target_pairs={{4,0},{8,4},{12,8},{16,12},{20,16},{24,20},{28,24},{5,1},{9,5},{13... | collective-permute-start | bytes 1572872 | tf_op jit(solution)/shard_map/ppermute | solution.py:26
  165.9 52.6 %copy-start.5 = (bf16[384,512]{1,0:T(8,128)(2,1)S(1)}, bf16[384,512]{1,0:T(8,128)(2,1)}, u32[]{:S(2)}) copy-start(bf16[384,512]{1,0:T(8,128)(2,1)} %fusion.60) | copy-start | bytes 1179652
  189.2 64.0 %all-gather.15.cloned.1.call-start = ((), (), s32[]{:S(2)}) async-start(), calls=%async_computation.4 | async-start | bytes 1966080 | tf_op jit(solution)/shard_map/all_gather | solution.py:224
  222.3 102.1 %all-gather.17.cloned.1.call-start = ((), (), s32[]{:S(2)}) async-start(), calls=%async_computation.5 | async-start | bytes 1966080 | tf_op jit(solution)/shard_map/all_gather | solution.py:234
  254.9 3.2 copy-start.1
  261.7 10.3 %collective-permute-start.4 = (bf16[256,1024]{1,0:T(8,128)(2,1)}, bf16[256,1024]{1,0:T(8,128)(2,1)S(1)}, u32[]{:S(2)}, u32[]{:S(2)}) collective-permute-start(bf16[256,1024]{1,0:T(8,128)(2,1)} %get-tuple-element.5), channel_id=1, source_target_pairs={{0,4},{4,8},{8,12},{12,16},{16,20},{20,24},{24,28},{1,5},{5,9},{9,... | collective-permute-start | bytes 1572872 | tf_op jit(solution)/shard_map/ppermute | solution.py:25
  265.6 10.6 %collective-permute-start.5 = (bf16[256,1024]{1,0:T(8,128)(2,1)S(1)}, bf16[256,1024]{1,0:T(8,128)(2,1)}, u32[]{:S(2)}, u32[]{:S(2)}) collective-permute-start(bf16[256,1024]{1,0:T(8,128)(2,1)S(1)} %get-tuple-element.6), channel_id=1, source_target_pairs={{4,0},{8,4},{12,8},{16,12},{20,16},{24,20},{28,24},{5,1},{9,5},{13... | collective-permute-start | bytes 1572872 | tf_op jit(solution)/shard_map/ppermute | solution.py:26
  271.6 52.7 %copy-start.4 = (bf16[384,512]{1,0:T(8,128)(2,1)S(1)}, bf16[384,512]{1,0:T(8,128)(2,1)}, u32[]{:S(2)}) copy-start(bf16[384,512]{1,0:T(8,128)(2,1)} %fusion.57) | copy-start | bytes 1179652
Sparse Core Ops, SparseCore 0:
  9.2 31.6 all-gather.6
  83.4 29.0 all-gather.8
  116.5 30.6 all-gather.10
  189.3 29.0 all-gather.12
  222.4 30.6 all-gather.14
  295.2 29.0 all-gather.16

commit v2 on v1

--- a/solution.py
+++ b/solution.py
@@ -180,66 +180,288 @@
     return first - row_base + reach, first - row_base - row + NA_ROWS - 1
 
 
-def attention_kernel(rows_dev, rows_all, q_ref, kv_ref, lanes_ref, out_ref, table):
-    width = q_ref.shape[1]
-    for pair in range(width // 128):
-        build_table(lambda off: lanes_ref[pair, off : off + 1, :], table)
-        cols = slice(pair * 128, (pair + 1) * 128)
-        vcols = slice(width + pair * 128, width + (pair + 1) * 128)
+MESH = pl.DeviceIdType.MESH
+
+
+def tp_copy(src, dst, sems, index, peer):
+    return pltpu.make_async_remote_copy(
+        src_ref=src,
+        dst_ref=dst,
+        send_sem=sems.at[0, index],
+        recv_sem=sems.at[1, index],
+        device_id=(lax.axis_index("sp"), peer),
+        device_id_type=MESH,
+    )
+
+
+class SquareGather:
+    def __init__(self, slots, sems, chunks):
+        self.slots, self.sems, self.chunks = slots, sems, chunks
+        self.rows = slots.shape[1] // chunks
+        self.me = lax.axis_index("tp")
+        self.across = self.me + 1 - 2 * (self.me % 2)
+        self.over = (self.me + 2) % 4
+        self.corner = (self.across + 2) % 4
+
+    def part(self, slot, chunk):
+        start = chunk * self.rows
+        if not isinstance(chunk, int):
+            start = pl.multiple_of(start, self.rows)
+        return self.slots.at[slot, pl.ds(start, self.rows), :]
+
+    def copy(self, kind, slot, chunk, peer):
+        part = self.part(slot, chunk)
+        return tp_copy(part, part, self.sems.at[kind], chunk, peer)
+
+    def send(self, chunk):
+        self.copy(0, self.me, chunk, self.across).start()
+        self.copy(1, self.me, chunk, self.over).start()
+
+    def relay(self, chunk):
+        self.copy(0, self.across, chunk, self.across).wait_recv()
+        self.copy(1, self.over, chunk, self.over).wait_recv()
+
+        @pl.when(chunk % 2 == 0)
+        def _():
+            self.copy(2, self.across, chunk, self.over).start()
+
+        @pl.when(chunk % 2 == 1)
+        def _():
+            self.copy(2, self.over, chunk, self.across).start()
+
+    def finish(self, chunk):
+        self.copy(2, self.corner, chunk, self.over).wait_recv()
+
+    def drain(self):
+        def one(chunk, carry):
+            self.copy(0, self.me, chunk, self.across).wait_send()
+            self.copy(1, self.me, chunk, self.over).wait_send()
+            self.copy(2, self.across, chunk, self.over).wait_send()
+            return carry
+
+        lax.fori_loop(0, self.chunks, one, 0)
+
+
+def stack_kernel(
+    rows_dev, rows_all,
+    x_ref, gain_ref, lanes_ref, wq_ref, wk_ref, wv_ref, wo_ref, out_ref,
+    gains, weights, stream, mixed, keyval, queries, normed, tables,
+    weight_sems, gain_sems, stream_sems, mixed_sems, halo_sems,
+):
+    sp, sp_size = lax.axis_index("sp"), lax.axis_size("sp")
+    layers = wq_ref.shape[0]
+    tokens, feats = x_ref.shape
+    width = feats
+    reach = NA_ROWS // 2 * GRID_W
+    streams = SquareGather(stream, stream_sems, rows_dev)
+    mixes = SquareGather(mixed, mixed_sems, rows_dev)
+    me, across, over = streams.me, streams.across, streams.over
+    corner = streams.corner
+    sources = (wk_ref, wv_ref, wq_ref, wo_ref)
+
+    def weight_copy(kind, layer):
+        return pltpu.make_async_copy(
+            sources[kind].at[layer], weights.at[kind, layer], weight_sems.at[kind, layer]
+        )
+
+    for layer in range(layers):
+        for kind in range(4):
+            weight_copy(kind, layer).start()
+
+    barrier = pltpu.get_barrier_semaphore()
+    for peer in (across, over, corner):
+        pl.semaphore_signal(barrier, inc=1, device_id=(sp, peer), device_id_type=MESH)
+
+    @pl.when(sp > 0)
+    def _():
+        pl.semaphore_signal(barrier, inc=1, device_id=(sp - 1, me), device_id_type=MESH)
+
+    @pl.when(sp < sp_size - 1)
+    def _():
+        pl.semaphore_signal(barrier, inc=1, device_id=(sp + 1, me), device_id_type=MESH)
+
+    stream[me] = x_ref[...]
+    gains[me] = gain_ref[...]
+    sides = jnp.minimum(sp, 1) + jnp.minimum(sp_size - 1 - sp, 1)
+    pl.semaphore_wait(barrier, 3 + sides)
+
+    def gain_copy(index, slot, peer):
+        return tp_copy(gains.at[slot], gains.at[slot], gain_sems, index, peer)
+
+    for index, peer in enumerate((across, over, corner)):
+        gain_copy(index, me, peer).start()
+    for index, peer in enumerate((across, over, corner)):
+        gain_copy(index, peer, peer).wait_recv()
+        gain_copy(index, me, peer).wait_send()
+
+    def halo_copy(parity, up):
+        src = keyval.at[parity, pl.ds(tokens if up else reach, reach), :]
+        dst = keyval.at[parity, pl.ds(0 if up else tokens + reach, reach), :]
+        return pltpu.make_async_remote_copy(
+            src_ref=src,
+            dst_ref=dst,
+            send_sem=halo_sems.at[0, parity, int(up)],
+            recv_sem=halo_sems.at[1, parity, int(up)],
+            device_id=(sp + 1 if up else sp - 1, me),
+            device_id_type=MESH,
+        )
+
+    def one_layer(layer, carry):
+        parity = layer % 2
+        for chunk in range(rows_dev):
+            streams.send(chunk)
+        for pair in range(width // 128):
+            build_table(
+                lambda off: lanes_ref[layer, pair, off : off + 1, :], tables.at[pair]
+            )
+
+        def relay_chunk(chunk, carry):
+            streams.relay(chunk)
+            return carry
+
+        lax.fori_loop(0, rows_dev, relay_chunk, 0)
+
+        def norm_chunk(chunk, carry):
+            streams.finish(chunk)
+            here = pl.ds(pl.multiple_of(chunk * GRID_W, GRID_W), GRID_W)
+            total = jnp.zeros((GRID_W, 1), jnp.float32)
+            for slot in range(4):
+                part = stream[slot, here, :].astype(jnp.float32)
+                total += jnp.sum(part * part, axis=1, keepdims=True)
+            inverse = lax.rsqrt(total * (1.0 / (4 * feats)) + epsilon)
+            for slot in range(4):
+                part = stream[slot, here, :].astype(jnp.float32)
+                gain = gains[slot, pl.ds(layer, 1), :]
+                normed[here, slot * feats : (slot + 1) * feats] = (
+                    part * inverse * gain
+                ).astype(jnp.bfloat16)
+            return carry
+
+        lax.fori_loop(0, rows_dev, norm_chunk, 0)
+        streams.drain()
+        for kind in range(2):
+            weight_copy(kind, layer).wait()
+            keyval[parity, reach : reach + tokens, kind * width : (kind + 1) * width] = contract(
+                normed[...], weights[kind, layer]
+            ).astype(jnp.bfloat16)
+
+        @pl.when(sp > 0)
+        def _():
+            halo_copy(parity, False).start()
+
+        @pl.when(sp < sp_size - 1)
+        def _():
+            halo_copy(parity, True).start()
+
+        weight_copy(2, layer).wait()
+        queries[...] = contract(normed[...], weights[2, layer]).astype(
+            jnp.bfloat16
+        ) * jnp.bfloat16(HEAD_DIM ** (-0.5))
+
+        @pl.when(sp > 0)
+        def _():
+            halo_copy(parity, True).wait_recv()
+
+        @pl.when(sp < sp_size - 1)
+        def _():
+            halo_copy(parity, False).wait_recv()
 
         def one_row(row, carry):
             start, off = row_window(row, rows_dev, rows_all)
             keys = pl.ds(pl.multiple_of(start * GRID_W, GRID_W), NA_ROWS * GRID_W)
             here = pl.ds(pl.multiple_of(row * GRID_W, GRID_W), GRID_W)
-            bias = table[pl.ds(pl.multiple_of(off * GRID_W, GRID_W), NA_ROWS * GRID_W), :]
-            out_ref[here, cols] = attend_row(
-                q_ref[here, cols], kv_ref[keys, cols], kv_ref[keys, vcols], bias
+            offs = pl.ds(pl.multiple_of(off * GRID_W, GRID_W), NA_ROWS * GRID_W)
+            for pair in range(width // 128):
+                cols = slice(pair * 128, (pair + 1) * 128)
+                vcols = slice(width + pair * 128, width + (pair + 1) * 128)
+                mixed[me, here, cols] = attend_row(
+                    queries[here, cols],
+                    keyval[parity, keys, cols],
+                    keyval[parity, keys, vcols],
+                    tables[pair, offs, :],
+                )
+            mixes.send(row)
+
+            @pl.when(row > 0)
+            def _():
+                mixes.relay(row - 1)
+
+            return carry
+
+        lax.fori_loop(0, rows_dev, one_row, 0)
+        mixes.relay(rows_dev - 1)
+
+        @pl.when(sp > 0)
+        def _():
+            halo_copy(parity, False).wait_send()
+
+        @pl.when(sp < sp_size - 1)
+        def _():
+            halo_copy(parity, True).wait_send()
+
+        def finish_chunk(chunk, carry):
+            mixes.finish(chunk)
+            return carry
+
+        lax.fori_loop(0, rows_dev, finish_chunk, 0)
+        mixes.drain()
+        weight_copy(3, layer).wait()
+        total = stream[me].astype(jnp.float32)
+        for slot in range(4):
+            total += contract(
+                mixed[slot], weights[3, layer, :, slot * width : (slot + 1) * width]
             )
-            return carry
-
-        lax.fori_loop(0, rows_dev, one_row, 0)
-
-
-def attention(queries, padded, lanes, rows_dev, rows_all):
+        stream[me] = total.astype(jnp.bfloat16)
+        return carry
+
+    lax.fori_loop(0, layers, one_layer, 0)
+    out_ref[...] = stream[me]
+
+
+def square_device(residual, norm_gain, w_query, w_key, w_value, w_out, offset_bias):
+    tokens, feats = residual.shape
+    layers = w_query.shape[0]
+    rows_dev = tokens // GRID_W
+    rows_all = rows_dev * lax.axis_size("sp")
+    lanes = bias_lanes(offset_bias)
+    gain = jnp.pad(norm_gain.astype(jnp.float32), ((0, 8 - layers), (0, 0)))
     vmem = pl.BlockSpec(memory_space=pltpu.VMEM)
+    hbm = pl.BlockSpec(memory_space=pl.ANY)
+    bf16, dma = jnp.bfloat16, pltpu.SemaphoreType.DMA
+    padded = tokens + NA_ROWS * GRID_W
     return pl.pallas_call(
-        lambda *refs: attention_kernel(rows_dev, rows_all, *refs),
-        out_shape=jax.ShapeDtypeStruct(queries.shape, jnp.bfloat16),
-        in_specs=[vmem] * 3,
+        lambda *refs: stack_kernel(rows_dev, rows_all, *refs),
+        out_shape=jax.ShapeDtypeStruct(residual.shape, bf16),
+        in_specs=[vmem] * 3 + [hbm] * 4,
         out_specs=vmem,
-        scratch_shapes=[pltpu.VMEM(((2 * NA_ROWS - 1) * GRID_W, 2 * GRID_W), jnp.float32)],
-        name="attention",
-    )(queries, padded, lanes)
-
-
-def paired_device(residual, norm_gain, w_query, w_key, w_value, w_out, offset_bias):
-    token_count = residual.shape[0]
-    rows_dev = token_count // GRID_W
-    rows_all = rows_dev * lax.axis_size("sp")
-    reach = NA_ROWS // 2
-    lanes = bias_lanes(offset_bias)
-    gains = lax.all_gather(norm_gain, "tp", axis=1, tiled=True).astype(jnp.float32)
-    stream = residual
-    for layer_index in range(LAYERS):
-        full_float = lax.all_gather(stream, "tp", axis=1, tiled=True).astype(jnp.float32)
-        inverse = lax.rsqrt(jnp.mean(full_float * full_float, axis=1, keepdims=True) + epsilon)
-        normed = (full_float * inverse * gains[layer_index][None, :]).astype(jnp.bfloat16)
-        keys = contract(normed, w_key[layer_index]).astype(jnp.bfloat16)
-        values = contract(normed, w_value[layer_index]).astype(jnp.bfloat16)
-        key_value = jnp.concatenate([keys, values], axis=1)
-        padded = padded_2(key_value, (("sp", 0),), reach * GRID_W)
-        queries = contract(normed, w_query[layer_index]).astype(jnp.bfloat16)
-        queries = queries * jnp.bfloat16(HEAD_DIM ** (-0.5))
-        attended = attention(queries, padded, lanes[layer_index], rows_dev, rows_all)
-        gathered = lax.all_gather(attended, "tp", axis=1, tiled=True)
-        mixed = contract(gathered, w_out[layer_index])
-        stream = (stream.astype(jnp.float32) + mixed).astype(jnp.bfloat16)
-    return stream
+        scratch_shapes=[
+            pltpu.VMEM((4, 8, feats), jnp.float32),
+            pltpu.VMEM((4,) + w_query.shape, bf16),
+            pltpu.VMEM((4, tokens, feats), bf16),
+            pltpu.VMEM((4, tokens, feats), bf16),
+            pltpu.VMEM((2, padded, 2 * feats), bf16),
+            pltpu.VMEM((tokens, feats), bf16),
+            pltpu.VMEM((tokens, 4 * feats), bf16),
+            pltpu.VMEM((feats // 128, (2 * NA_ROWS - 1) * GRID_W, 128), jnp.float32),
+            dma((4, layers)),
+            dma((2, 3)),
+            dma((3, 2, rows_dev)),
+            dma((3, 2, rows_dev)),
+            dma((2, 2, 2)),
+        ],
+        compiler_params=pltpu.CompilerParams(
+            collective_id=0, has_side_effects=True, vmem_limit_bytes=56 * 1024 * 1024
+        ),
+        name="stack",
+    )(residual, gain, lanes, w_query, w_key, w_value, w_out)
 
 
 def per_device(residual, norm_gain, w_query, w_key, w_value, w_out, offset_bias):
-    fits = offset_bias.shape[1] % 2 == 0 and 2 * HEAD_DIM == 128 and 2 * GRID_W == 128
-    body = paired_device if fits else generic_device
+    paired = offset_bias.shape[1] % 2 == 0 and 2 * HEAD_DIM == 128 and 2 * GRID_W == 128
+    square = lax.axis_size("tp") == 4 and offset_bias.shape[1] * HEAD_DIM == residual.shape[1]
+    body = generic_device
+    if paired and square:
+        body = square_device
     return body(residual, norm_gain, w_query, w_key, w_value, w_out, offset_bias)
 
 

time: 338 us -> 145 us (0.43)
  waiting for transfers between devices: 190 us -> 0 us
  Pallas kernels: 49.2 us -> 139 us
  matrix products: 39.1 us -> 0 us
  starting transfers between devices: 17.6 us -> 0 us
  other arithmetic: 15.9 us -> 1.29 us
  between operations: 13.7 us -> 0.03 us
  blocking collectives: 6.17 us -> 0 us
    all_gather x6 -> x0, waiting for transfers between devices: 175 us -> none  [the longest x3 87.8 us: paired_device(): lax.all_gather(stream, 'tp', axis=1, tiled=True).astype(jnp.float32)]
    pallas_call x3 -> x1, Pallas kernels: 49.2 us -> 139 us  [square_device(): pl.pallas_call(lambda *refs: stack_kernel(rows_dev, rows_all, *refs), out...]
    dot_general x12 -> x0, matrix products: 39.1 us -> none  [contract(): lax.dot_general(left, right, (((1,), (1,)), ((), ())), preferred_element_...]
    ppermute x6 -> x0, starting transfers between devices: 17.4 us -> none  [the longest x3 11.5 us: padded_2(): before = lax.ppermute(last, axis, up)]
    ppermute x6 -> x0, waiting for transfers between devices: 13.7 us -> none  [the longest x3 12.8 us: padded_2(): after = lax.ppermute(first, axis, down)]
    concatenate x6 -> x0, other arithmetic: 10.5 us -> none  [the longest x3 7.46 us: padded_2(): array = jnp.concatenate([before, array, after], axis=dim)]
    all_gather x1 -> x0, blocking collectives: 6.17 us -> none  [paired_device(): lax.all_gather(norm_gain, 'tp', axis=1, tiled=True).astype(jnp.float32)]
    reduce_sum x3 -> x0, other arithmetic: 5.37 us -> none  [paired_device(): jnp.mean(full_float * full_float, axis=1, keepdims=True) + epsilon]
  transfers between devices with their start and end apart: 12 -> 0, of which waited for: 12 -> 0; matrix products, arithmetic and copies ran while one was open for 4% -> 0% of each run, Pallas kernels for 0% -> 0%
where the time goes in v2:
time: 145 us; the launch traced here: 144 us
  Pallas kernels  139 us (96%)
  local copies, waits for them, and re-layouts  3.69 us (3%)
    pallas_call x1, Pallas kernels, square_device(): pl.pallas_call(lambda *refs: stack_kernel(rows_dev, rows_all, *refs), out...  139 us

profile of v2, /device:TPU:11, one launch (start us, length us, event | category | flops | bytes accessed | tf_op | source)
XLA Modules:
  0.0 144.4 jit_solution(8316273039218775465)
XLA Ops:
  0.0 1.3 pad_convert_fusion.refs_1_
  1.3 1.0 rev.4
  2.4 0.1 copy.10
  2.4 0.8 reshape.7.refs_2_
  3.2 139.4 %stack.1 = bf16[384,512]{1,0:T(8,128)(2,1)} custom-call(bf16[384,512]{1,0:T(8,128)(2,1)} %refs_0_.1, f32[8,512]{1,0:T(8,128)} %pad_convert_fusion.refs_1_, f32[3,4,16,128]{3,2,1,0:T(8,128)} %reshape.7.refs_2_, bf16[3,512,2048]{2,1,0:T(8,128)(2,1)} %refs_3_.1, bf16[3,512,2048]{2,1,0:T(8,128)(2,1)} %refs_4_.1, bf16[3,512,2048]{2,1,0:T(8,128)(2,1)} %refs_5_.1, ...), custom_call_target="tpu_custom_call" | custom-call | tf_op jit(solution)/shard_map/stack/pallas_call | solution.py:432
  142.6 1.8 %copy.12 = bf16[384,512]{1,0:T(8,128)(2,1)} copy(bf16[384,512]{1,0:T(8,128)(2,1)} %stack.1) | data formatting | bytes 786432
  (1 shorter events, 0.0 us)

commit v3 on v2

--- a/solution.py
+++ b/solution.py
@@ -181,6 +181,7 @@
 
 
 MESH = pl.DeviceIdType.MESH
+LAG = 3
 
 
 def tp_copy(src, dst, sems, index, peer):
@@ -246,7 +247,7 @@
     rows_dev, rows_all,
     x_ref, gain_ref, lanes_ref, wq_ref, wk_ref, wv_ref, wo_ref, out_ref,
     gains, weights, stream, mixed, keyval, queries, normed, tables,
-    weight_sems, gain_sems, stream_sems, mixed_sems, halo_sems,
+    partial, weight_sems, gain_sems, stream_sems, mixed_sems, halo_sems,
 ):
     sp, sp_size = lax.axis_index("sp"), lax.axis_size("sp")
     layers = wq_ref.shape[0]
@@ -281,7 +282,7 @@
         pl.semaphore_signal(barrier, inc=1, device_id=(sp + 1, me), device_id_type=MESH)
 
     stream[me] = x_ref[...]
-    gains[me] = gain_ref[...]
+    gains[me, 0:layers, :] = gain_ref[...].astype(jnp.float32)
     sides = jnp.minimum(sp, 1) + jnp.minimum(sp_size - 1 - sp, 1)
     pl.semaphore_wait(barrier, 3 + sides)
 
@@ -290,41 +291,57 @@
 
     for index, peer in enumerate((across, over, corner)):
         gain_copy(index, me, peer).start()
-    for index, peer in enumerate((across, over, corner)):
-        gain_copy(index, peer, peer).wait_recv()
-        gain_copy(index, me, peer).wait_send()
-
-    def halo_copy(parity, up):
-        src = keyval.at[parity, pl.ds(tokens if up else reach, reach), :]
-        dst = keyval.at[parity, pl.ds(0 if up else tokens + reach, reach), :]
+
+    pairs = rows_dev // 2
+    tall = 2 * GRID_W
+    parts = NA_ROWS // 4
+    down_parts = range(parts)
+    up_parts = range(pairs - parts, pairs)
+    order = sorted(range(pairs), key=lambda j: -((j in down_parts) + (j in up_parts)))
+
+    def halo_copy(parity, up, part, kind):
+        cols = slice(kind * width, (kind + 1) * width)
+        local = reach + (pairs - parts + part if up else part) * tall
+        there = part * tall + (0 if up else tokens + reach)
         return pltpu.make_async_remote_copy(
-            src_ref=src,
-            dst_ref=dst,
-            send_sem=halo_sems.at[0, parity, int(up)],
-            recv_sem=halo_sems.at[1, parity, int(up)],
+            src_ref=keyval.at[parity, pl.ds(local, tall), cols],
+            dst_ref=keyval.at[parity, pl.ds(there, tall), cols],
+            send_sem=halo_sems.at[0, parity, int(up), part, kind],
+            recv_sem=halo_sems.at[1, parity, int(up), part, kind],
             device_id=(sp + 1 if up else sp - 1, me),
             device_id_type=MESH,
         )
 
+    def send_halo(parity, pair, kind):
+        if pair in down_parts:
+
+            @pl.when(sp > 0)
+            def _():
+                halo_copy(parity, False, pair, kind).start()
+
+        if pair in up_parts:
+
+            @pl.when(sp < sp_size - 1)
+            def _():
+                halo_copy(parity, True, pair - (pairs - parts), kind).start()
+
     def one_layer(layer, carry):
         parity = layer % 2
-        for chunk in range(rows_dev):
-            streams.send(chunk)
+        for pair in order[:2]:
+            streams.send(2 * pair)
+            streams.send(2 * pair + 1)
         for pair in range(width // 128):
             build_table(
                 lambda off: lanes_ref[layer, pair, off : off + 1, :], tables.at[pair]
             )
 
-        def relay_chunk(chunk, carry):
-            streams.relay(chunk)
-            return carry
-
-        lax.fori_loop(0, rows_dev, relay_chunk, 0)
-
-        def norm_chunk(chunk, carry):
-            streams.finish(chunk)
-            here = pl.ds(pl.multiple_of(chunk * GRID_W, GRID_W), GRID_W)
-            total = jnp.zeros((GRID_W, 1), jnp.float32)
+        def relay_pair(pair):
+            streams.relay(2 * pair)
+            streams.relay(2 * pair + 1)
+
+        def norm_pair(pair):
+            here = slice(pair * tall, (pair + 1) * tall)
+            total = jnp.zeros((tall, 1), jnp.float32)
             for slot in range(4):
                 part = stream[slot, here, :].astype(jnp.float32)
                 total += jnp.sum(part * part, axis=1, keepdims=True)
@@ -335,36 +352,50 @@
                 normed[here, slot * feats : (slot + 1) * feats] = (
                     part * inverse * gain
                 ).astype(jnp.bfloat16)
-            return carry
-
-        lax.fori_loop(0, rows_dev, norm_chunk, 0)
+
+        def project_pair(pair):
+            here = slice(pair * tall, (pair + 1) * tall)
+            there = slice(reach + pair * tall, reach + (pair + 1) * tall)
+            for kind in range(2):
+                keyval[parity, there, kind * width : (kind + 1) * width] = contract(
+                    normed[here, :], weights[kind, layer]
+                ).astype(jnp.bfloat16)
+                send_halo(parity, pair, kind)
+            queries[here, :] = contract(normed[here, :], weights[2, layer]).astype(
+                jnp.bfloat16
+            ) * jnp.bfloat16(HEAD_DIM ** (-0.5))
+
+        @pl.when(layer == 0)
+        def _():
+            for index, peer in enumerate((across, over, corner)):
+                gain_copy(index, peer, peer).wait_recv()
+                gain_copy(index, me, peer).wait_send()
+
+        for kind in range(3):
+            weight_copy(kind, layer).wait()
+        relay_pair(order[0])
+        for pair in order[2:]:
+            streams.send(2 * pair)
+            streams.send(2 * pair + 1)
+        for place, pair in enumerate(order):
+            if place + 1 < pairs:
+                relay_pair(order[place + 1])
+            streams.finish(2 * pair)
+            streams.finish(2 * pair + 1)
+            norm_pair(pair)
+            project_pair(pair)
         streams.drain()
-        for kind in range(2):
-            weight_copy(kind, layer).wait()
-            keyval[parity, reach : reach + tokens, kind * width : (kind + 1) * width] = contract(
-                normed[...], weights[kind, layer]
-            ).astype(jnp.bfloat16)
-
-        @pl.when(sp > 0)
-        def _():
-            halo_copy(parity, False).start()
-
-        @pl.when(sp < sp_size - 1)
-        def _():
-            halo_copy(parity, True).start()
-
-        weight_copy(2, layer).wait()
-        queries[...] = contract(normed[...], weights[2, layer]).astype(
-            jnp.bfloat16
-        ) * jnp.bfloat16(HEAD_DIM ** (-0.5))
-
-        @pl.when(sp > 0)
-        def _():
-            halo_copy(parity, True).wait_recv()
-
-        @pl.when(sp < sp_size - 1)
-        def _():
-            halo_copy(parity, False).wait_recv()
+
+        for part in range(parts):
+            for kind in range(2):
+
+                @pl.when(sp > 0)
+                def _():
+                    halo_copy(parity, True, part, kind).wait_recv()
+
+                @pl.when(sp < sp_size - 1)
+                def _():
+                    halo_copy(parity, False, part, kind).wait_recv()
 
         def one_row(row, carry):
             start, off = row_window(row, rows_dev, rows_all)
@@ -382,22 +413,38 @@
                 )
             mixes.send(row)
 
-            @pl.when(row > 0)
+            @pl.when(row >= LAG)
             def _():
-                mixes.relay(row - 1)
+                mixes.relay(row - LAG)
 
             return carry
 
         lax.fori_loop(0, rows_dev, one_row, 0)
-        mixes.relay(rows_dev - 1)
-
-        @pl.when(sp > 0)
-        def _():
-            halo_copy(parity, False).wait_send()
-
-        @pl.when(sp < sp_size - 1)
-        def _():
-            halo_copy(parity, True).wait_send()
+
+        def relay_rest(row, carry):
+            mixes.relay(row)
+            return carry
+
+        lax.fori_loop(rows_dev - LAG, rows_dev, relay_rest, 0)
+        weight_copy(3, layer).wait()
+
+        def out_part(slot):
+            cols = pl.ds(pl.multiple_of(slot * width, width), width)
+            return contract(mixed[slot], weights[3, layer, :, cols])
+
+        total = stream[me].astype(jnp.float32) + out_part(me)
+        partial[...] = total + out_part(across) + out_part(over)
+
+        for part in range(parts):
+            for kind in range(2):
+
+                @pl.when(sp > 0)
+                def _():
+                    halo_copy(parity, False, part, kind).wait_send()
+
+                @pl.when(sp < sp_size - 1)
+                def _():
+                    halo_copy(parity, True, part, kind).wait_send()
 
         def finish_chunk(chunk, carry):
             mixes.finish(chunk)
@@ -405,12 +452,7 @@
 
         lax.fori_loop(0, rows_dev, finish_chunk, 0)
         mixes.drain()
-        weight_copy(3, layer).wait()
-        total = stream[me].astype(jnp.float32)
-        for slot in range(4):
-            total += contract(
-                mixed[slot], weights[3, layer, :, slot * width : (slot + 1) * width]
-            )
+        total = partial[...] + out_part(corner)
         stream[me] = total.astype(jnp.bfloat16)
         return carry
 
@@ -424,7 +466,6 @@
     rows_dev = tokens // GRID_W
     rows_all = rows_dev * lax.axis_size("sp")
     lanes = bias_lanes(offset_bias)
-    gain = jnp.pad(norm_gain.astype(jnp.float32), ((0, 8 - layers), (0, 0)))
     vmem = pl.BlockSpec(memory_space=pltpu.VMEM)
     hbm = pl.BlockSpec(memory_space=pl.ANY)
     bf16, dma = jnp.bfloat16, pltpu.SemaphoreType.DMA
@@ -435,7 +476,7 @@
         in_specs=[vmem] * 3 + [hbm] * 4,
         out_specs=vmem,
         scratch_shapes=[
-            pltpu.VMEM((4, 8, feats), jnp.float32),
+            pltpu.VMEM((4, -(-layers // 8) * 8, feats), jnp.float32),
             pltpu.VMEM((4,) + w_query.shape, bf16),
             pltpu.VMEM((4, tokens, feats), bf16),
             pltpu.VMEM((4, tokens, feats), bf16),
@@ -443,24 +484,27 @@
             pltpu.VMEM((tokens, feats), bf16),
             pltpu.VMEM((tokens, 4 * feats), bf16),
             pltpu.VMEM((feats // 128, (2 * NA_ROWS - 1) * GRID_W, 128), jnp.float32),
+            pltpu.VMEM((tokens, feats), jnp.float32),
             dma((4, layers)),
             dma((2, 3)),
             dma((3, 2, rows_dev)),
             dma((3, 2, rows_dev)),
-            dma((2, 2, 2)),
+            dma((2, 2, 2, NA_ROWS // 4, 2)),
         ],
         compiler_params=pltpu.CompilerParams(
             collective_id=0, has_side_effects=True, vmem_limit_bytes=56 * 1024 * 1024
         ),
         name="stack",
-    )(residual, gain, lanes, w_query, w_key, w_value, w_out)
+    )(residual, norm_gain, lanes, w_query, w_key, w_value, w_out)
 
 
 def per_device(residual, norm_gain, w_query, w_key, w_value, w_out, offset_bias):
     paired = offset_bias.shape[1] % 2 == 0 and 2 * HEAD_DIM == 128 and 2 * GRID_W == 128
     square = lax.axis_size("tp") == 4 and offset_bias.shape[1] * HEAD_DIM == residual.shape[1]
+    rows_dev = residual.shape[0] // GRID_W
+    even = rows_dev % 2 == 0 and rows_dev >= NA_ROWS // 2
     body = generic_device
-    if paired and square:
+    if paired and square and even:
         body = square_device
     return body(residual, norm_gain, w_query, w_key, w_value, w_out, offset_bias)
 

time: 145 us -> 120 us (0.83)
  Pallas kernels: 139 us -> 115 us
    pallas_call x1, Pallas kernels: 139 us -> 115 us  [square_device(): pl.pallas_call(lambda *refs: stack_kernel(rows_dev, rows_all, *refs), out...]
where the time goes in v3:
time: 120 us; the launch traced here: 118 us
  Pallas kernels  115 us (96%)
  local copies, waits for them, and re-layouts  3.69 us (3%)
    pallas_call x1, Pallas kernels, square_device(): pl.pallas_call(lambda *refs: stack_kernel(rows_dev, rows_all, *refs), out...  115 us

profile of v3, /device:TPU:11, one launch (start us, length us, event | category | flops | bytes accessed | tf_op | source)
XLA Modules:
  0.0 118.2 jit_solution(1794046354901854105)
XLA Ops:
  0.0 1.0 rev.4
  1.1 0.1 copy.10
  1.2 0.8 reshape.7.refs_2_
  2.0 114.5 %stack.1 = bf16[384,512]{1,0:T(8,128)(2,1)} custom-call(bf16[384,512]{1,0:T(8,128)(2,1)} %refs_0_.1, bf16[3,512]{1,0:T(4,128)(2,1)} %refs_1_.1, f32[3,4,16,128]{3,2,1,0:T(8,128)} %reshape.7.refs_2_, bf16[3,512,2048]{2,1,0:T(8,128)(2,1)} %refs_3_.1, bf16[3,512,2048]{2,1,0:T(8,128)(2,1)} %refs_4_.1, bf16[3,512,2048]{2,1,0:T(8,128)(2,1)} %refs_5_.1, ...), custom_call_target="tpu_custom_call" | custom-call | tf_op jit(solution)/shard_map/stack/pallas_call | solution.py:473
  116.5 1.8 %copy.12 = bf16[384,512]{1,0:T(8,128)(2,1)} copy(bf16[384,512]{1,0:T(8,128)(2,1)} %stack.1) | data formatting | bytes 786432
  (1 shorter events, 0.0 us)

commit v4 on v3

--- a/solution.py
+++ b/solution.py
@@ -386,18 +386,26 @@
             project_pair(pair)
         streams.drain()
 
-        for part in range(parts):
-            for kind in range(2):
-
-                @pl.when(sp > 0)
-                def _():
-                    halo_copy(parity, True, part, kind).wait_recv()
-
-                @pl.when(sp < sp_size - 1)
-                def _():
-                    halo_copy(parity, False, part, kind).wait_recv()
-
-        def one_row(row, carry):
+        def wait_halo(up):
+            for part in range(parts):
+                for kind in range(2):
+                    halo_copy(parity, up, part, kind).wait_recv()
+
+        @pl.when(sp < sp_size - 1)
+        def _():
+            wait_halo(False)
+
+        @pl.when((sp > 0) & (sp == sp_size - 1))
+        def _():
+            wait_halo(True)
+
+        def one_row(step, carry):
+            row = rows_dev - 1 - step
+
+            @pl.when((step == rows_dev - NA_ROWS // 2) & (sp > 0) & (sp < sp_size - 1))
+            def _():
+                wait_halo(True)
+
             start, off = row_window(row, rows_dev, rows_all)
             keys = pl.ds(pl.multiple_of(start * GRID_W, GRID_W), NA_ROWS * GRID_W)
             here = pl.ds(pl.multiple_of(row * GRID_W, GRID_W), GRID_W)
@@ -413,16 +421,16 @@
                 )
             mixes.send(row)
 
-            @pl.when(row >= LAG)
+            @pl.when(step >= LAG)
             def _():
-                mixes.relay(row - LAG)
+                mixes.relay(row + LAG)
 
             return carry
 
         lax.fori_loop(0, rows_dev, one_row, 0)
 
-        def relay_rest(row, carry):
-            mixes.relay(row)
+        def relay_rest(step, carry):
+            mixes.relay(rows_dev - 1 - step)
             return carry
 
         lax.fori_loop(rows_dev - LAG, rows_dev, relay_rest, 0)

time: 120 us -> 118 us (0.983)
  Pallas kernels: 115 us -> 113 us
    pallas_call x1, Pallas kernels: 115 us -> 113 us  [square_device(): pl.pallas_call(lambda *refs: stack_kernel(rows_dev, rows_all, *refs), out...]
where the time goes in v4:
time: 118 us; the launch traced here: 116 us
  Pallas kernels  113 us (96%)
  local copies, waits for them, and re-layouts  3.69 us (3%)
    pallas_call x1, Pallas kernels, square_device(): pl.pallas_call(lambda *refs: stack_kernel(rows_dev, rows_all, *refs), out...  113 us

profile of v4, /device:TPU:11, one launch (start us, length us, event | category | flops | bytes accessed | tf_op | source)
XLA Modules:
  0.0 116.5 jit_solution(17833300808582484427)
XLA Ops:
  0.0 1.0 rev.4
  1.1 0.1 copy.10
  1.2 0.8 reshape.7.refs_2_
  2.0 112.7 %stack.1 = bf16[384,512]{1,0:T(8,128)(2,1)} custom-call(bf16[384,512]{1,0:T(8,128)(2,1)} %refs_0_.1, bf16[3,512]{1,0:T(4,128)(2,1)} %refs_1_.1, f32[3,4,16,128]{3,2,1,0:T(8,128)} %reshape.7.refs_2_, bf16[3,512,2048]{2,1,0:T(8,128)(2,1)} %refs_3_.1, bf16[3,512,2048]{2,1,0:T(8,128)(2,1)} %refs_4_.1, bf16[3,512,2048]{2,1,0:T(8,128)(2,1)} %refs_5_.1, ...), custom_call_target="tpu_custom_call" | custom-call | tf_op jit(solution)/shard_map/stack/pallas_call | solution.py:481
  114.7 1.8 %copy.12 = bf16[384,512]{1,0:T(8,128)(2,1)} copy(bf16[384,512]{1,0:T(8,128)(2,1)} %stack.1) | data formatting | bytes 786432
  (1 shorter events, 0.0 us)

commit v5 on v4

--- a/solution.py
+++ b/solution.py
@@ -325,11 +325,15 @@
             def _():
                 halo_copy(parity, True, pair - (pairs - parts), kind).start()
 
+    def send_pair(pair):
+        streams.send(2 * pair)
+        streams.send(2 * pair + 1)
+
+    for pair in order[:2]:
+        send_pair(pair)
+
     def one_layer(layer, carry):
         parity = layer % 2
-        for pair in order[:2]:
-            streams.send(2 * pair)
-            streams.send(2 * pair + 1)
         for pair in range(width // 128):
             build_table(
                 lambda off: lanes_ref[layer, pair, off : off + 1, :], tables.at[pair]
@@ -460,8 +464,17 @@
 
         lax.fori_loop(0, rows_dev, finish_chunk, 0)
         mixes.drain()
-        total = partial[...] + out_part(corner)
-        stream[me] = total.astype(jnp.bfloat16)
+        corner_cols = pl.ds(pl.multiple_of(corner * width, width), width)
+        for place, pair in enumerate(order):
+            here = slice(pair * tall, (pair + 1) * tall)
+            last = contract(mixed[corner, here, :], weights[3, layer, :, corner_cols])
+            stream[me, here, :] = (partial[here, :] + last).astype(jnp.bfloat16)
+            if place < 2:
+
+                @pl.when(layer < layers - 1)
+                def _():
+                    send_pair(pair)
+
         return carry
 
     lax.fori_loop(0, layers, one_layer, 0)

time: 118 us -> 118 us (level)
  no operation moved by 1% of the time
where the time goes in v5:
time: 118 us; the launch traced here: 117 us
  Pallas kernels  113 us (96%)
  local copies, waits for them, and re-layouts  3.69 us (3%)
    pallas_call x1, Pallas kernels, square_device(): pl.pallas_call(lambda *refs: stack_kernel(rows_dev, rows_all, *refs), out...  113 us

profile of v5, /device:TPU:11, one launch (start us, length us, event | category | flops | bytes accessed | tf_op | source)
XLA Modules:
  0.0 116.8 jit_solution(8289379475213109125)
XLA Ops:
  0.0 1.0 rev.4
  1.1 0.1 copy.10
  1.2 0.8 reshape.7.refs_2_
  2.0 113.1 %stack.1 = bf16[384,512]{1,0:T(8,128)(2,1)} custom-call(bf16[384,512]{1,0:T(8,128)(2,1)} %refs_0_.1, bf16[3,512]{1,0:T(4,128)(2,1)} %refs_1_.1, f32[3,4,16,128]{3,2,1,0:T(8,128)} %reshape.7.refs_2_, bf16[3,512,2048]{2,1,0:T(8,128)(2,1)} %refs_3_.1, bf16[3,512,2048]{2,1,0:T(8,128)(2,1)} %refs_4_.1, bf16[3,512,2048]{2,1,0:T(8,128)(2,1)} %refs_5_.1, ...), custom_call_target="tpu_custom_call" | custom-call | tf_op jit(solution)/shard_map/stack/pallas_call | solution.py:494
  115.1 1.8 %copy.12 = bf16[384,512]{1,0:T(8,128)(2,1)} copy(bf16[384,512]{1,0:T(8,128)(2,1)} %stack.1) | data formatting | bytes 786432
  (1 shorter events, 0.0 us)
